TPU v7x, 1024 devices: a whole 4x4x32 slice. The times are simulated.
1024 devices in a mesh: sp: 256 (over z, x, core), tp: 4 (over y).
Axes of the slice: x: 4, y: 4, z: 32, core: 2. Of those that a mesh axis runs over, the one named last changes fastest.
Arguments:
- proj_value: bfloat16 [98304, 1024], P('sp', 'tp'), may hold values from -6 to 6
- proj_gate: bfloat16 [98304, 1024], P('sp', 'tp'), may hold values from -8 to 8
- out_cotangent: bfloat16 [98304, 2048], P('sp'), may hold values from -24 to 24
- out_weight: bfloat16 [1024, 2048], P('tp'), may hold values from -0.1875 to 0.1875
- conv_taps: bfloat16 [31, 1024], P(None, 'tp'), may hold values from -1 to 1
- norm_gain: float32 [1024], P('tp'), may hold values from 0.1 to 1.9
- row_mean: float32 [98304], P('sp'), may hold values from -2 to 2
- row_scale: float32 [98304], P('sp'), may hold values from 0.7 to 3
Outputs:
- value_grad: bfloat16 [98304, 1024], P('sp', 'tp')
- gate_grad: bfloat16 [98304, 1024], P('sp', 'tp')
- out_weight_grad: float32 [2048, 1024], P('sp', 'tp')
- taps_grad: float32 [31, 1024], P(None, 'tp')
- gain_grad: float32 [1024], P('tp')
All inputs are finite; a program needn't handle non-finite values.
Results may differ from a plain program's by a relative error of at most 0.0047.
Values may be sent and summed in bfloat16 or wider, within the bound.
A program may use at most 32 MiB of HBM per device.

v0:
```python
import jax
import jax.numpy as jnp
from jax import lax
from jax.sharding import Mesh
from jax.sharding import PartitionSpec as P

SP = ("sp_0", "sp_1", "sp_2")


def shifted(value, axis, steps):
    count = lax.axis_size(axis)
    first, last = (max(0, -steps), min(count, count - steps))
    return lax.ppermute(value, axis, [(source, source + steps) for source in range(first, last)])


def own_block(parts, axes, sequence):
    inside = parts.shape[1:]
    parts = parts.reshape(*(lax.axis_size(a) for a in axes), *inside)
    parts = jnp.moveaxis(parts, sequence, range(len(axes))).reshape(-1, *inside)
    for k in sequence:
        parts = lax.psum_scatter(parts, axes[k], scatter_dimension=0, tiled=True)
    return parts[0]


def in_blocks(array, dim, devices):
    lengths = array.shape
    parts = array.reshape(*lengths[:dim], devices, lengths[dim] // devices, *lengths[dim + 1 :])
    return jnp.moveaxis(parts, dim, 0)


def sum_by_axis(array, axes, sequence, dim):
    devices = lax.axis_size(axes)
    return own_block(in_blocks(array, dim, devices), axes, sequence)


def from_everyone(array, axis):
    devices = lax.axis_size(axis)
    return lax.all_to_all(
        jnp.broadcast_to(array[None], (devices, *array.shape)), axis, 0, 0, tiled=True
    )


def over_copies(array, axis):
    return from_everyone(array, axis).sum(axis=0)


def in_one(arrays, axis):
    ends = [0]
    for a in arrays:
        ends.append(ends[-1] + a.size)
    running = over_copies(jnp.concatenate([a.ravel() for a in arrays]), axis)
    return tuple((running[b:e].reshape(a.shape) for a, b, e in zip(arrays, ends, ends[1:])))


def over_axes(array, axes):
    for axis in axes:
        array = lax.psum(array, axis)
    return array


def shards(
    proj_value, proj_gate, out_cotangent, out_weight, conv_taps, norm_gain, row_mean, row_scale
):
    kernel = conv_taps.shape[0]
    margin = kernel - 1
    length = proj_value.shape[0]
    channels = proj_value.shape[1]
    gate_sig = jax.nn.sigmoid(proj_gate.astype(jnp.float32))
    gated = (proj_value.astype(jnp.float32) * gate_sig).astype(jnp.bfloat16)
    before = shifted(gated[length - margin :], SP, 1)
    padded = jnp.concatenate([before, gated], 0).astype(jnp.float32)
    taps_wide = conv_taps.astype(jnp.float32)
    conv = jnp.zeros((length, channels), jnp.float32)
    for offset in range(kernel):
        conv = conv + taps_wide[offset][None, :] * padded[offset : offset + length]
    normed = (conv - row_mean[:, None]) * row_scale[:, None]
    active = normed * norm_gain[None, :]
    sig_act = jax.nn.sigmoid(active)
    hidden = (active * sig_act).astype(jnp.bfloat16)
    upstream = lax.dot_general(
        out_cotangent, out_weight, (((1,), (1,)), ((), ())), preferred_element_type=jnp.float32
    )
    weight_grad = sum_by_axis(
        lax.dot_general(
            out_cotangent, hidden, (((0,), (0,)), ((), ())), preferred_element_type=jnp.float32
        ),
        SP,
        (2, 0, 1),
        0,
    )
    d_active = upstream * sig_act * (1.0 + active * (1.0 - sig_act))
    gain_local = jnp.sum(d_active * normed, 0)
    d_normed = d_active * norm_gain[None, :]
    sum_first, sum_second = in_one((jnp.sum(d_normed, 1), jnp.sum(d_normed * normed, 1)), "tp")
    total_channels = channels * lax.axis_size("tp")
    first = sum_first / total_channels
    second = sum_second / total_channels
    d_conv = row_scale[:, None] * (d_normed - first[:, None] - normed * second[:, None])
    taps_local = jnp.stack(
        [jnp.sum(d_conv * padded[offset : offset + length], 0) for offset in range(kernel)]
    )
    taps_grad, gain_grad = (over_axes(taps_local, SP), over_axes(gain_local, SP))
    spread = jnp.zeros((length + margin, channels), jnp.float32)
    for offset in range(kernel):
        placed = taps_wide[offset][None, :] * d_conv
        spread = spread + jnp.pad(placed, ((offset, margin - offset), (0, 0)))
    arrived = shifted(spread[:margin], SP, -1)
    tail_part = jnp.concatenate([jnp.zeros((length - margin, channels), jnp.float32), arrived], 0)
    d_gated = spread[margin:] + tail_part
    value_grad = (d_gated * gate_sig).astype(jnp.bfloat16)
    gate_grad = (d_gated * proj_value.astype(jnp.float32) * gate_sig * (1.0 - gate_sig)).astype(
        jnp.bfloat16
    )
    return (value_grad, gate_grad, weight_grad, taps_grad, gain_grad)


def solution(mesh):
    split = Mesh(mesh.devices.reshape(32, 4, 2, mesh.shape["tp"]), ("sp_0", "sp_1", "sp_2", "tp"))
    placed = (
        P(SP, "tp"),
        P(SP, "tp"),
        P(SP, None),
        P("tp", None),
        P(None, "tp"),
        P("tp"),
        P(SP),
        P(SP),
    )
    return jax.shard_map(
        shards,
        mesh=split,
        in_specs=placed,
        out_specs=(P(SP, "tp"), P(SP, "tp"), P(SP, "tp"), P(None, "tp"), P("tp")),
        check_vma=False,
    )
```

profile of v0, /device:TPU:1, one launch (start us, length us, event | category | flops | bytes accessed | tf_op | source)
XLA Modules:
  0.0 247.0 jit_solution(1409863044858874739)
XLA Ops:
  7.2 0.0 copy-start
  7.2 0.0 reduce-scatter.4.cloned.1.call-start
  7.2 1.2 fusion.1
  8.5 4.5 %collective-permute-start = (bf16[30,256]{1,0:T(8,128)(2,1)S(1)}, bf16[30,256]{1,0:T(8,128)(2,1)S(1)}, u32[]{:S(2)}, u32[]{:S(2)}) collective-permute-start(bf16[30,256]{1,0:T(8,128)(2,1)S(1)} %slice.331), channel_id=1, source_target_pairs={{0,4},{4,8},{8,12},{12,16},{16,20},{20,24},{24,28},{28,32},{32,36}... | collective-permute-start | bytes 46088 | tf_op jit(solution)/shard_map/ppermute | solution.py:13
  13.0 1.0 fusion.8
  14.0 1.0 fusion.9
  15.0 9.6 %collective-permute-done = bf16[30,256]{1,0:T(8,128)(2,1)S(1)} collective-permute-done((bf16[30,256]{1,0:T(8,128)(2,1)S(1)}, bf16[30,256]{1,0:T(8,128)(2,1)S(1)}, u32[]{:S(2)}, u32[]{:S(2)}) %collective-permute-start) | collective-permute-done | bytes 15392 | tf_op jit(solution)/shard_map/ppermute | solution.py:13
  24.6 0.0 copy-start.3
  24.6 1.8 subtract_multiply_fusion.1
  26.4 0.0 copy-done
  26.4 0.0 copy-done.3
  26.4 2.1 convolution_bitcast_fusion
  28.5 2.9 %copy.20 = f32[2048,256]{1,0:T(8,128)} copy(f32[2048,256]{0,1:T(8,128)} %convolution_bitcast_fusion) | data formatting | bytes 4194304 | tf_op jit(solution)/shard_map/dot_general | solution.py:84
  31.4 3.2 %copy.21 = f32[2,32,4,8,256]{4,3,2,1,0:T(8,128)} copy(f32[2,32,4,8,256]{4,3,0,2,1:T(8,128)} %bitcast.73) | data formatting | bytes 4194304 | tf_op jit(solution)/shard_map/transpose | solution.py:19
  34.6 0.0 reduce-scatter.4.cloned.1.call-update
  34.6 0.0 copy-start.4
  34.7 0.0 copy-start.5
  34.7 0.0 reduce-scatter.6.cloned.1.call-start
  34.7 2.0 multiply_reduce_fusion
  36.8 6.5 %all_to_all.6 = f32[4,1,768]{2,1,0:T(1,128)S(1)} all-to-all(f32[4,1,768]{2,1,0:T(1,128)S(1)} %broadcast_in_dim.2), channel_id=1, replica_groups=mesh['sp_0'=32,'sp_1'=4,'sp_2'=2,'tp'=4] {'tp'}, dimensions={0} | all-to-all | bytes 24576 | tf_op jit(solution)/shard_map/all_to_all | solution.py:38
  43.3 22.6 %reduce-scatter.4.cloned.1.call-done = f32[128,8,256]{2,1,0:T(8,128)} async-done(((f32[256,8,256]{2,1,0:T(8,128)}), f32[128,8,256]{2,1,0:T(8,128)}) %reduce-scatter.4.cloned.1.call-update) | async-done | bytes 1048592 | tf_op jit(solution)/shard_map/reduce_scatter | solution.py:21
  65.9 0.0 reduce-scatter.6.cloned.1.call-update
  65.9 0.0 reduce-scatter.8.cloned.1.call-start
  66.0 0.0 copy-done.4
  66.0 0.0 copy-done.5
  66.0 3.3 %multiply_reduce_fusion.1 = (f32[256]{0:T(256)S(1)}, f32[256]{0:T(256)S(1)}, f32[256]{0:T(256)S(1)}, f32[256]{0:T(256)S(1)}, f32[256]{0:T(256)S(1)}, /*index=5*/...) fusion(f32[414,256]{1,0:T(8,128)S(1)} %maximum_convert_fusion, ...), kind=kLoop, calls=%fused_computation.12 | loop fusion | flops 10219008 | bytes 13033472 | tf_op jit(solution)/shard_map/reduce_sum | solution.py:100
  69.3 0.3 broadcast_multiply_fusion.29
  69.6 0.6 multiply_reduce_fusion.19
  70.2 0.8 broadcast_multiply_fusion.30
  71.0 0.0 copy-start.1
  71.0 0.0 copy-start.2
  71.0 1.3 pad_add_fusion
  72.3 1.9 collective-permute-start.1
  74.3 0.1 stack.127
  74.4 85.7 %all-reduce.32 = (f32[31,256]{1,0:T(8,128)S(1)}, f32[256]{0:T(256)S(1)}) all-reduce(f32[31,256]{1,0:T(8,128)S(1)} %stack.127, f32[256]{0:T(256)S(1)} %get-tuple-element.36), channel_id=1, replica_groups=mesh['sp_0'=32,'sp_1'=4,'sp_2'=2,'tp'=4] {'sp_0'}, use_global_device_ids=true, to_apply=%region_37.0 | all-reduce | flops 8192 | bytes 65536 | tf_op jit(solution)/shard_map/psum | solution.py:57
  160.0 13.6 %all-reduce.33 = (f32[31,256]{1,0:T(8,128)S(1)}, f32[256]{0:T(256)S(1)}) all-reduce(f32[31,256]{1,0:T(8,128)S(1)} %get-tuple-element.39, f32[256]{0:T(256)S(1)} %get-tuple-element.40), channel_id=1, replica_groups=mesh['sp_0'=32,'sp_1'=4,'sp_2'=2,'tp'=4] {'sp_1'}, use_global_device_ids=true, to_apply=%region_38.0 | all-reduce | flops 8192 | bytes 65536 | tf_op jit(solution)/shard_map/psum | solution.py:57
  173.6 31.3 %all-reduce.34 = (f32[31,256]{1,0:T(8,128)}, f32[256]{0:T(256)}) all-reduce(f32[31,256]{1,0:T(8,128)S(1)} %get-tuple-element.41, f32[256]{0:T(256)S(1)} %get-tuple-element.42), channel_id=1, replica_groups=mesh['sp_0'=32,'sp_1'=4,'sp_2'=2,'tp'=4] {'sp_2'}, use_global_device_ids=true, to_apply=%region_39.0 | all-reduce | flops 8192 | bytes 65536 | tf_op jit(solution)/shard_map/psum | solution.py:57
  205.0 0.0 reduce-scatter.6.cloned.1.call-done
  205.0 0.0 reduce-scatter.8.cloned.1.call-update
  205.0 0.0 collective-permute-done.1
  205.0 0.0 copy-done.1
  205.0 0.0 copy-done.2
  205.0 0.9 fusion.4
  206.0 34.5 %reduce-scatter.8.cloned.1.call-done = f32[1,8,256]{2,1,0:T(8,128)} async-done(((f32[4,8,256]{2,1,0:T(8,128)}), f32[1,8,256]{2,1,0:T(8,128)}) %reduce-scatter.8.cloned.1.call-update) | async-done | bytes 8208 | tf_op jit(solution)/shard_map/reduce_scatter | solution.py:21
  (7 shorter events, 0.1 us)
Async XLA Ops:
  7.2 19.2 %copy-start = (bf16[384,2048]{1,0:T(8,128)(2,1)S(1)}, bf16[384,2048]{1,0:T(8,128)(2,1)}, u32[]{:S(2)}) copy-start(bf16[384,2048]{1,0:T(8,128)(2,1)} %param.10) | copy-start | bytes 4718596
  7.2 58.7 %reduce-scatter.4.cloned.1.call-start = ((), (), s32[]{:S(2)}) async-start(), calls=%async_computation.4 | async-start | bytes 3145728 | tf_op jit(solution)/shard_map/reduce_scatter | solution.py:21
  8.5 16.1 %collective-permute-start = (bf16[30,256]{1,0:T(8,128)(2,1)S(1)}, bf16[30,256]{1,0:T(8,128)(2,1)S(1)}, u32[]{:S(2)}, u32[]{:S(2)}) collective-permute-start(bf16[30,256]{1,0:T(8,128)(2,1)S(1)} %slice.331), channel_id=1, source_target_pairs={{0,4},{4,8},{8,12},{12,16},{16,20},{20,24},{24,28},{28,32},{32,36}... | collective-permute-start | bytes 46088 | tf_op jit(solution)/shard_map/ppermute | solution.py:13
  24.6 1.8 copy-start.3
  34.6 31.3 %copy-start.4 = (f32[384]{0:T(512)S(1)}, f32[384]{0:T(512)}, u32[]{:S(2)}) copy-start(f32[384]{0:T(512)} %param.14) | copy-start | bytes 4612
  34.7 31.3 %copy-start.5 = (f32[384]{0:T(512)S(1)}, f32[384]{0:T(512)}, u32[]{:S(2)}) copy-start(f32[384]{0:T(512)} %param.15) | copy-start | bytes 4612
  34.7 170.3 %reduce-scatter.6.cloned.1.call-start = ((), (), s32[]{:S(2)}) async-start(), calls=%async_computation.5 | async-start | bytes 1081344 | tf_op jit(solution)/shard_map/reduce_scatter | solution.py:21
  65.9 174.6 %reduce-scatter.8.cloned.1.call-start = ((), (), s32[]{:S(2)}) async-start(), calls=%async_computation.6 | async-start | bytes 40960 | tf_op jit(solution)/shard_map/reduce_scatter | solution.py:21
  71.0 134.0 %copy-start.1 = (bf16[384,256]{1,0:T(8,128)(2,1)S(1)}, bf16[384,256]{1,0:T(8,128)(2,1)}, u32[]{:S(2)}) copy-start(bf16[384,256]{1,0:T(8,128)(2,1)} %param.8) | copy-start | bytes 589828
  71.0 134.0 %copy-start.2 = (bf16[384,256]{1,0:T(8,128)(2,1)S(1)}, bf16[384,256]{1,0:T(8,128)(2,1)}, u32[]{:S(2)}) copy-start(bf16[384,256]{1,0:T(8,128)(2,1)} %param.9) | copy-start | bytes 589828
  72.3 132.7 %collective-permute-start.1 = (f32[30,256]{1,0:T(8,128)S(1)}, f32[30,256]{1,0:T(8,128)S(1)}, u32[]{:S(2)}, u32[]{:S(2)}) collective-permute-start(f32[30,256]{1,0:T(8,128)S(1)} %slice.394), channel_id=1, source_target_pairs={{4,0},{8,4},{12,8},{16,12},{20,16},{24,20},{28,24},{32,28},{36,32}... | collective-permute-start | bytes 92168 | tf_op jit(solution)/shard_map/ppermute | solution.py:13
Sparse Core Ops, SparseCore 0:
  34.8 31.0 reduce-scatter.3
  69.2 112.8 reduce-scatter.5
  205.1 35.3 reduce-scatter.7
where the time goes:
time: 249 us; the launch traced here: 247 us
  blocking collectives  137 us (55%)
  waiting for transfers between devices  66.7 us (27%)
  between operations  14 us (6%)
  other arithmetic  10.3 us (4%)
  local copies, waits for them, and re-layouts  8.29 us (3%)
  starting transfers between devices  6.54 us (3%)
  matrix products  4.08 us (2%)
    psum x3, blocking collectives, over_axes(): array = lax.psum(array, axis)  131 us
    reduce_scatter x3, waiting for transfers between devices, own_block(): parts = lax.psum_scatter(parts, axes[k], scatter_dimension=0, tiled=True)  57.1 us
    ppermute x2, waiting for transfers between devices, shifted(): lax.ppermute(value, axis, [(source, source + steps) for source in range(f...  9.58 us
    all_to_all x1, blocking collectives, from_everyone(): lax.all_to_all(jnp.broadcast_to(array[None], (devices, *array.shape)), ax...  6.53 us
    ppermute x2, starting transfers between devices, shifted(): lax.ppermute(value, axis, [(source, source + steps) for source in range(f...  6.42 us
  transfers between devices with their start and end apart: 5, of which 3 were waited for; matrix products, arithmetic and copies ran while one was open for 5% of the time, Pallas kernels for 0%

commit v1 on v0

v1 whole, which is shorter than its diff:
```python
import functools

import jax
import jax.numpy as jnp
from jax import lax
from jax.experimental import pallas as pl
from jax.experimental.pallas import tpu as pltpu
from jax.sharding import Mesh
from jax.sharding import PartitionSpec as P

MESH = pl.DeviceIdType.MESH
SP = ("z", "x", "c")
NZ, NX, NC, NY = 32, 4, 2, 4
F32, BF16 = jnp.float32, jnp.bfloat16
HALO = 32
NEAR = 4
CHUNKS = 4


def sigmoid(v):
    return 1.0 / (1.0 + jnp.exp(-v))


def main_kernel(
    pv_h, pg_h, cot_h, ow_h, taps_h, gain_h, mean_h, scale_h,
    vg_o, gg_o, wg_o, tg_o, gn_o,
    pv, pg, cot, ow, taps_b, gain_v, mean_v, scale_v,
    hs, hr, gp, sg, us, cv, nm, dn, hid, dcp, rm, rs, s1, s2, wt, gacc,
    ys, yr, tacc, tp, tr, tz, tf, w32, wc, wo, xs, xr, zs, zo, zr,
    in_sem, halo_sem, dhalo_sem, y_ss, y_rs, t_ss, t_rs, tz_ss, tz_rs, tf_ss, tf_rs,
    c_ss, c_rs, x_ss, x_rs, z_ss, z_rs, far_sem,
):
    length = pv.shape[0]
    taps = taps_b.shape[0]
    z, x, c, y = (lax.axis_index(a) for a in ("z", "x", "c", "y"))
    j_me = x * NC + c
    rem, div = lax.rem, lax.div

    def copy_in(src, dst, k):
        cp = pltpu.make_async_copy(src, dst, in_sem.at[k])
        cp.start()
        return cp

    in_pv = copy_in(pv_h, pv, 0)
    in_pg = copy_in(pg_h, pg, 1)
    in_small = [copy_in(s, d, 2 + k) for k, (s, d) in enumerate(
        ((taps_h, taps_b), (gain_h, gain_v), (mean_h, mean_v), (scale_h, scale_v)))]
    in_ow = copy_in(ow_h, ow, 6)
    part = length // 3
    in_cot = [copy_in(cot_h.at[pl.ds(part * k, part), :], cot.at[pl.ds(part * k, part), :], 7 + k) for k in range(3)]

    plane = []
    for q in range(1, NX * NC):
        plane.append((rem(x + q // NC, NX), rem(c + q % NC, NC)))
    xs_of = [rem(x + q, NX) for q in range(1, NX)]
    nxt = {"z": rem(z + div(x + c, NX), NZ), "x": rem(x + c, NX), "c": 1 - c}
    nxt["z"] = rem(z + div(x * NC + c + 1, NX * NC), NZ)
    prv = {"z": rem(z + NZ - 1 + div(x + NX - 1 + c, NX), NZ), "x": rem(x + NX - 1 + c, NX), "c": 1 - c}

    barrier = pltpu.get_barrier_semaphore()
    near = [{"x": px, "c": pc} for px, pc in plane] + [{"y": rem(y + q, NY)} for q in range(1, NY)] + [nxt, prv]
    near += [{"z": rem(z + q, NZ)} for q in range(1, NEAR + 1)] + [{"z": rem(z + NZ - q, NZ)} for q in range(1, NEAR + 1)]
    for to in near:
        pl.semaphore_signal(barrier, inc=1, device_id=to, device_id_type=MESH)

    in_pv.wait()
    in_pg.wait()

    def gate_rows(r0, rows):
        for h in range(2):
            lanes = pl.ds(128 * h, 128)
            s = sigmoid(pg[pl.ds(r0, rows), lanes].astype(F32))
            g = (pv[pl.ds(r0, rows), lanes].astype(F32) * s).astype(BF16)
            sg[h, pl.ds(r0, rows), :] = s
            gp[h, pl.ds(r0 + HALO, rows), :] = g.astype(F32)
            yield lanes, g

    for lanes, g in gate_rows(length - HALO, HALO):
        hs[:, lanes] = g
    pl.semaphore_wait(barrier, len(near))
    halo = pltpu.make_async_remote_copy(hs, hr, halo_sem.at[0], halo_sem.at[1], device_id=nxt, device_id_type=MESH)
    halo.start()

    @pl.loop(0, (length - HALO) // 32)
    def _(i):
        for _ in gate_rows(pl.multiple_of(i * 32, 32), 32):
            pass

    for cp in in_small:
        cp.wait()
    for h in range(2):
        wt[h, 0:taps, :] = taps_b[:, pl.ds(128 * h, 128)].astype(F32)
    gain = [gain_v[pl.ds(128 * h, 128)].reshape(1, 128) for h in range(2)]
    for b in range(length // 128):
        rows = pl.ds(128 * b, 128)
        rm[rows, :] = jnp.broadcast_to(mean_v[rows].reshape(1, 128), (128, 128)).T
        rs[rows, :] = jnp.broadcast_to(scale_v[rows].reshape(1, 128), (128, 128)).T

    in_ow.wait()
    for k, cp in enumerate(in_cot):
        cp.wait()
        rows = pl.ds(part * k, part)
        u = lax.dot_general(cot[rows, :], ow[...], (((1,), (1,)), ((), ())), preferred_element_type=F32)
        for h in range(2):
            us[h, rows, :] = u[:, 128 * h:128 * h + 128]

    def conv_rows(h, r0, rows):
        acc = jnp.zeros((rows, 128), F32)
        for k in range(taps):
            acc = acc + wt[h, k:k + 1, :] * gp[h, pl.ds(r0 + (HALO + 1 - taps + k), rows), :]
        cv[h, pl.ds(r0, rows), :] = acc

    def point_rows(r0, rows):
        sl = pl.ds(r0, rows)
        sums = []
        for h in range(2):
            n = (cv[h, sl, :] - rm[sl, :]) * rs[sl, :]
            a = n * gain[h]
            s = sigmoid(a)
            hid[sl, pl.ds(128 * h, 128)] = (a * s).astype(BF16)
            da = us[h, sl, :] * s * (1.0 + a * (1.0 - s))
            d = da * gain[h]
            dan = da * n
            gacc[h, :, :] += dan.reshape(rows // 8, 8, 128).sum(axis=0)
            nm[h, sl, :] = n
            dn[h, sl, :] = d
            sums.append((d, dan * gain[h]))
        s1[sl, :] = sums[0][0] + sums[1][0]
        s2[sl, :] = sums[0][1] + sums[1][1]

    gacc[...] = jnp.zeros_like(gacc)

    @pl.loop(0, 8)
    def _(i):
        conv_rows(rem(i, 2), pl.multiple_of(HALO + div(i, 2) * 88, 8), 88)

    @pl.loop(0, (length - HALO) // 32)
    def _(i):
        point_rows(pl.multiple_of(HALO + i * 32, 32), 32)

    def row_sums(b):
        rows = pl.ds(128 * b, 128)
        ys[0:1, rows] = jnp.sum(s1[rows, :].T, axis=0, keepdims=True)
        ys[1:2, rows] = jnp.sum(s2[rows, :].T, axis=0, keepdims=True)

    row_sums(1)
    row_sums(2)

    def far(step, k):
        for to in (rem(z + step, NZ), rem(z + NZ - step, NZ)):
            pl.semaphore_signal(far_sem.at[k], inc=1, device_id={"z": to}, device_id_type=MESH)

    far(NEAR, 0)

    halo.wait_recv()
    first_dev = (z * (NX * NC) + j_me) == 0
    for h in range(2):
        got = hr[:, pl.ds(128 * h, 128)].astype(F32)
        gp[h, 0:HALO, :] = jnp.where(first_dev, jnp.zeros_like(got), got)
        conv_rows(h, 0, HALO)
    point_rows(0, HALO)
    row_sums(0)

    y_cp = []
    yr[y] = ys[...]
    for q in range(1, NY):
        y_cp.append(pltpu.make_async_remote_copy(
            ys, yr.at[y], y_ss.at[q], y_rs.at[q], device_id={"y": rem(y + q, NY)}, device_id_type=MESH))
        y_cp[-1].start()

    pl.semaphore_wait(far_sem.at[0], 2)
    far(2 * NEAR, 1)

    zc = NZ // CHUNKS
    c_cp = []
    for k in range(CHUNKS):
        @pl.loop(0, zc // 2)
        def _(i):
            lanes = pl.ds(pl.multiple_of((k * (zc // 2) + i) * 128, 128), 128)
            w = lax.dot_general(cot[:, lanes], hid[...], (((0,), (0,)), ((), ())), preferred_element_type=F32)
            for e in range(2):
                for px in range(NX):
                    for pc in range(NC):
                        r = 64 * e + 16 * px + 8 * pc
                        for h in range(2):
                            w32[k, pc, px, 2 * i + e, h, :, :] = w[r:r + 8, 128 * h:128 * h + 128]
        c_cp.append(pltpu.make_async_remote_copy(
            w32.at[k, 1 - c], wc.at[k], c_ss.at[k], c_rs.at[k], device_id={"c": 1 - c}, device_id_type=MESH))
        c_cp[-1].start()

    x_cp = []

    def x_phase(k):
        c_cp[k].wait_recv()

        @pl.loop(0, NX * zc)
        def _(i):
            px, e = div(i, zc), rem(i, zc)
            v = (w32[k, c, px, e] + wc[k, px, e]).reshape(16, 128)
            xs[k, px, e] = v.astype(BF16)

            @pl.when(px == x)
            def _():
                wo[k * zc + e] = v
        for q in (2, 1, 3):
            to = rem(x + q, NX)
            x_cp.append(pltpu.make_async_remote_copy(
                xs.at[k, to], xr.at[q - 1, k], x_ss.at[q, k], x_rs.at[q, k], device_id={"x": to}, device_id_type=MESH))
            x_cp[-1].start()

    x_phase(0)
    x_phase(1)

    for cp in y_cp:
        cp.wait_recv()
    inv = 1.0 / (NY * pv.shape[1])
    tot = ((yr[0] + yr[1]) + (yr[2] + yr[3])) * inv
    for b in range(length // 128):
        rows = pl.ds(128 * b, 128)
        s1[rows, :] = jnp.broadcast_to(tot[0:1, 128 * b:128 * b + 128], (128, 128)).T
        s2[rows, :] = jnp.broadcast_to(tot[1:2, 128 * b:128 * b + 128], (128, 128)).T

    @pl.loop(0, length // 32)
    def _(i):
        sl = pl.ds(pl.multiple_of(i * 32, 32), 32)
        for h in range(2):
            dcp[h, sl, :] = rs[sl, :] * (dn[h, sl, :] - s1[sl, :] - nm[h, sl, :] * s2[sl, :])

    dhalo = pltpu.make_async_remote_copy(
        dcp.at[:, pl.ds(0, HALO), :], dcp.at[:, pl.ds(length, HALO), :], dhalo_sem.at[0], dhalo_sem.at[1],
        device_id=prv, device_id_type=MESH)
    dhalo.start()

    for h in range(2):
        def tap_rows(i, acc):
            r0 = pl.multiple_of(i * 8, 8)
            d = dcp[h, pl.ds(r0, 8), :]
            return tuple(acc[k] + d * gp[h, pl.ds(r0 + (HALO + 1 - taps + k), 8), :] for k in range(taps))
        acc = lax.fori_loop(0, length // 8, tap_rows, tuple(jnp.zeros((8, 128), F32) for _ in range(taps)))
        for k in range(taps):
            tp[k // 4, 4 * h + k % 4, :] = jnp.sum(acc[k], axis=0)
        tp[taps // 4, 4 * h + taps % 4, :] = jnp.sum(gacc[h], axis=0)

    t_cp = []
    tr[j_me] = tp[j_me]
    for q, (px, pc) in enumerate(plane):
        t_cp.append(pltpu.make_async_remote_copy(
            tp.at[px * NC + pc], tr.at[j_me], t_ss.at[q], t_rs.at[q], device_id={"x": px, "c": pc}, device_id_type=MESH))
        t_cp[-1].start()

    pl.semaphore_wait(far_sem.at[1], 2)
    x_phase(2)
    x_phase(3)

    for cp in t_cp:
        cp.wait_recv()
    share = tr[0]
    for j in range(1, NX * NC):
        share = share + tr[j]
    tz[z] = share
    tf[0] = share

    def z_copy(src, dst, ss, rs_, d):
        return pltpu.make_async_remote_copy(
            src, dst, ss.at[d], rs_.at[d], device_id={"z": rem(z + d, NZ)}, device_id_type=MESH)

    def by_distance(i):
        half = div(i + 1, 2)
        return NZ // 2 + half * (1 - 2 * rem(i, 2))

    @pl.loop(0, NZ - 1)
    def _(i):
        d = by_distance(i)
        z_copy(tf.at[0], tz.at[z], tz_ss, tz_rs, d).start()

    for cp in x_cp:
        cp.wait_recv()

    @pl.loop(0, NZ)
    def _(i):
        k, e = div(i, zc), rem(i, zc)
        v = wo[i] + (xr[0, k, e].astype(F32) + xr[1, k, e].astype(F32)) + xr[2, k, e].astype(F32)
        zs[i] = v.astype(BF16)

        @pl.when(i == z)
        def _():
            zo[...] = v

    @pl.loop(0, NZ - 1)
    def _(i):
        d = by_distance(i)
        z_copy(zs.at[rem(z + d, NZ)], zr.at[z], z_ss, z_rs, d).start()

    last_dev = (z * (NX * NC) + j_me) == NZ * NX * NC - 1
    dhalo.wait_recv()
    for h in range(2):
        got = dcp[h, pl.ds(length, HALO), :]
        dcp[h, pl.ds(length, HALO), :] = jnp.where(last_dev, jnp.zeros_like(got), got)

    for h in range(2):
        @pl.loop(0, length // 64)
        def _(i):
            r0 = pl.multiple_of(i * 64, 64)
            acc = jnp.zeros((64, 128), F32)
            for k in range(taps):
                acc = acc + wt[h, k:k + 1, :] * dcp[h, pl.ds(r0 + (taps - 1 - k), 64), :]
            sl, lanes = pl.ds(r0, 64), pl.ds(128 * h, 128)
            s = sg[h, sl, :]
            vg_o[sl, lanes] = (acc * s).astype(BF16)
            gg_o[sl, lanes] = (acc * pv[sl, lanes].astype(F32) * s * (1.0 - s)).astype(BF16)

    @pl.loop(1, NZ)
    def _(d):
        z_copy(tf.at[0], tz.at[z], tz_ss, tz_rs, d).wait_recv()

    total = lax.fori_loop(1, NZ, lambda i, a: a + tz[i], tz[0])
    tr[j_me] = total
    f_cp = []
    for q, (px, pc) in enumerate(plane):
        f_cp.append(pltpu.make_async_remote_copy(
            tr.at[j_me], tacc.at[j_me], tf_ss.at[q], tf_rs.at[q], device_id={"x": px, "c": pc}, device_id_type=MESH))
        f_cp[-1].start()
    tacc[j_me] = total

    @pl.loop(1, NZ)
    def _(d):
        z_copy(zs.at[0], zr.at[z], z_ss, z_rs, d).wait_recv()
    zr[z] = jnp.zeros((16, 128), BF16)
    wsum = lax.fori_loop(0, NZ, lambda i, a: a + zr[i].astype(F32), zo[...])
    for h in range(2):
        wg_o[:, pl.ds(128 * h, 128)] = wsum[8 * h:8 * h + 8, :]

    for cp in f_cp:
        cp.wait_recv()
    for j in range(NX * NC):
        t = tacc[j]
        for h in range(2):
            for i in range(4):
                row = t[4 * h + i:4 * h + i + 1, :]
                if 4 * j + i < taps:
                    tg_o[4 * j + i:4 * j + i + 1, pl.ds(128 * h, 128)] = row
                else:
                    gn_o[pl.ds(128 * h, 128)] = row.reshape(128)

    halo.wait_send()
    dhalo.wait_send()
    for cp in y_cp + c_cp + x_cp + t_cp + f_cp:
        cp.wait_send()

    @pl.loop(1, NZ)
    def _(d):
        z_copy(tf.at[0], tz.at[z], tz_ss, tz_rs, d).wait_send()
        z_copy(zs.at[0], zr.at[z], z_ss, z_rs, d).wait_send()


def shards(pv, pg, cot, ow, taps, gain, mean, scale):
    length, ch = pv.shape
    d = cot.shape[1]
    zc = NZ // CHUNKS
    V, D = pltpu.VMEM, pltpu.SemaphoreType.DMA
    any_spec, vmem = pl.BlockSpec(memory_space=pl.ANY), pl.BlockSpec(memory_space=pltpu.VMEM)
    scratch = [
        V((length, ch), BF16), V((length, ch), BF16), V((length, d), BF16), V((ch, d), BF16),
        V(taps.shape, BF16), V((ch,), F32), V((length,), F32), V((length,), F32),
        V((HALO, ch), BF16), V((HALO, ch), BF16),
        V((2, length + HALO, 128), F32), V((2, length, 128), F32), V((2, length, 128), F32),
        V((2, length, 128), F32), V((2, length, 128), F32), V((2, length, 128), F32),
        V((length, ch), BF16), V((2, length + HALO, 128), F32),
        V((length, 128), F32), V((length, 128), F32), V((length, 128), F32), V((length, 128), F32),
        V((2, 32, 128), F32), V((2, 8, 128), F32),
        V((2, length), F32), V((NY, 2, length), F32),
        V((8, 8, 128), F32), V((8, 8, 128), F32), V((8, 8, 128), F32), V((NZ, 8, 128), F32), V((1, 8, 128), F32),
        V((CHUNKS, NC, NX, zc, 2, 8, 128), F32), V((CHUNKS, NX, zc, 2, 8, 128), F32),
        V((NZ, 16, 128), F32), V((CHUNKS, NX, zc, 16, 128), BF16), V((NX - 1, CHUNKS, zc, 16, 128), BF16),
        V((NZ, 16, 128), BF16), V((16, 128), F32), V((NZ, 16, 128), BF16),
        D((10,)), D((2,)), D((2,)), D((NY,)), D((NY,)), D((7,)), D((7,)), D((NZ,)), D((NZ,)), D((7,)), D((7,)),
        D((CHUNKS,)), D((CHUNKS,)), D((NX, CHUNKS)), D((NX, CHUNKS)), D((NZ,)), D((NZ,)),
        pltpu.SemaphoreType.REGULAR((2,)),
    ]
    return pl.pallas_call(
        main_kernel,
        out_shape=(
            jax.ShapeDtypeStruct((length, ch), BF16), jax.ShapeDtypeStruct((length, ch), BF16),
            jax.ShapeDtypeStruct((8, ch), F32), jax.ShapeDtypeStruct(taps.shape, F32), jax.ShapeDtypeStruct((ch,), F32),
        ),
        in_specs=[any_spec] * 8,
        out_specs=(vmem,) * 5,
        scratch_shapes=scratch,
        name="conv_back",
        compiler_params=pltpu.CompilerParams(collective_id=0, has_side_effects=True, vmem_limit_bytes=56 * 2**20),
    )(pv, pg, cot, ow, taps, gain, mean, scale)


def solution(mesh):
    split = Mesh(mesh.devices.reshape(NZ, NX, NC, mesh.shape["tp"]), ("z", "x", "c", "y"))
    placed = (P(SP, "y"), P(SP, "y"), P(SP, None), P("y", None), P(None, "y"), P("y"), P(SP), P(SP))
    return jax.shard_map(
        shards, mesh=split, in_specs=placed,
        out_specs=(P(SP, "y"), P(SP, "y"), P(SP, "y"), P(None, "y"), P("y")), check_vma=False,
    )
```

time: 249 us -> 77.9 us (0.31)
  the two profiles are of different devices: /device:TPU:1 before, /device:TPU:24 now
where the time goes in v1:
time: 77.9 us; the launch traced here: 77.6 us
  Pallas kernels  69.8 us (90%)
  local copies, waits for them, and re-layouts  7.14 us (9%)
    pallas_call x1, Pallas kernels, shards(): pl.pallas_call(main_kernel, out_shape=(jax.ShapeDtypeStruct((length, ch),...  69.8 us
    unnamed x5, local copies, waits for them, and re-layouts  7.14 us

profile of v1, /device:TPU:24, one launch (start us, length us, event | category | flops | bytes accessed | tf_op | source)
XLA Modules:
  0.0 77.6 jit_solution(3996671023682633116)
XLA Ops:
  0.6 69.8 %conv_back.1 = (bf16[384,256]{1,0:T(8,128)(2,1)}, bf16[384,256]{1,0:T(8,128)(2,1)}, f32[8,256]{1,0:T(8,128)}, f32[31,256]{1,0:T(8,128)}, f32[256]{0:T(256)}) custom-call(bf16[384,256]{1,0:T(8,128)(2,1)} %pv_h.1, bf16[384,256]{1,0:T(8,128)(2,1)} %pg_h.1, bf16[384,2048]{1,0:T(8,128)(2,1)} %cot_h.1, bf16[256,2048]{1,0:T(8,128)(2,1)} %ow_h.1, ...), custom_call_target="tpu_custom_call" | custom-call | tf_op jit(solution)/shard_map/conv_back/pallas_call | solution.py:380
  70.5 1.6 %copy.18 = bf16[384,256]{1,0:T(8,128)(2,1)} copy(bf16[384,256]{1,0:T(8,128)(2,1)} %get-tuple-element.10) | data formatting | bytes 393216
  72.1 1.6 %copy.19 = bf16[384,256]{1,0:T(8,128)(2,1)} copy(bf16[384,256]{1,0:T(8,128)(2,1)} %get-tuple-element.11) | data formatting | bytes 393216
  73.7 1.3 %copy.20 = f32[8,256]{1,0:T(8,128)} copy(f32[8,256]{1,0:T(8,128)} %get-tuple-element.12) | data formatting | bytes 16384
  75.0 1.4 %copy.21 = f32[31,256]{1,0:T(8,128)} copy(f32[31,256]{1,0:T(8,128)} %get-tuple-element.13) | data formatting | bytes 63488
  76.4 1.2 %copy.22 = f32[256]{0:T(256)} copy(f32[256]{0:T(256)} %get-tuple-element.14) | data formatting | bytes 2048

commit v2 on v1

v2 whole, which is shorter than its diff:
```python
import functools

import jax
import jax.numpy as jnp
from jax import lax
from jax.experimental import pallas as pl
from jax.experimental.pallas import tpu as pltpu
from jax.sharding import Mesh
from jax.sharding import PartitionSpec as P

MESH = pl.DeviceIdType.MESH
SP = ("z", "x", "c")
NZ, NX, NC, NY = 32, 4, 2, 4
F32, BF16 = jnp.float32, jnp.bfloat16
HALO = 32
NEAR = 2
NH = NZ // 2
CHUNKS = 4
HC = NH // CHUNKS


def sigmoid(v):
    return 1.0 / (1.0 + jnp.exp(-v))


def main_kernel(
    pv_h, pg_h, cot_h, ow_h, taps_h, gain_h, mean_h, scale_h,
    vg_o, gg_o, wg_o, tg_o, gn_o,
    pv, pg, cot, ow, taps_b, gain_v, mean_v, scale_v,
    hs, hr, gp, sg, us, cv, nm, dn, hid, dcp, rm, rs, s1, s2, wt, gacc,
    cot_t, ys, yr, kacc, tacc, tp, tr, tz, tf, w32, wc, xs, xr, zs, zo, zr,
    in_sem, halo_sem, dhalo_sem, y_ss, y_rs, t_ss, t_rs, tz_ss, tz_rs, tf_ss, tf_rs,
    c_ss, c_rs, x_ss, x_rs, z_ss, z_rs, far_sem,
):
    length = pv.shape[0]
    taps = taps_b.shape[0]
    blocks = length // 128
    z, x, c, y = (lax.axis_index(a) for a in ("z", "x", "c", "y"))
    rem, div = lax.rem, lax.div
    zh, zp = div(z, 2), rem(z, 2)
    m_me = (zp * NX + x) * NC + c

    def copy_in(src, dst, k):
        cp = pltpu.make_async_copy(src, dst, in_sem.at[k])
        cp.start()
        return cp

    in_pv = copy_in(pv_h, pv, 0)
    in_pg = copy_in(pg_h, pg, 1)
    in_small = [copy_in(s, d, 2 + k) for k, (s, d) in enumerate(
        ((taps_h, taps_b), (gain_h, gain_v), (mean_h, mean_v), (scale_h, scale_v)))]
    in_ow = copy_in(ow_h, ow, 6)
    part = length // 3
    in_cot = [copy_in(cot_h.at[pl.ds(part * k, part), :], cot.at[pl.ds(part * k, part), :], 7 + k) for k in range(3)]

    mates = []
    for dx in (2, 1, 3, 0):
        for dz in range(2):
            for dc in range(NC):
                if dx or dz or dc:
                    mates.append((rem(zp + dz, 2), rem(x + dx, NX), rem(c + dc, NC)))
    wmates = []
    for dx in (2, 1, 3, 0):
        for dz in range(2):
            if dx or dz:
                wmates.append((rem(zp + dz, 2), rem(x + dx, NX), dz * NX + dx - 1))

    def mate(pz, px, pc):
        return {"z": 2 * zh + pz, "x": px, "c": pc}

    nxt = {"z": rem(z + div(x * NC + c + 1, NX * NC), NZ), "x": rem(x + c, NX), "c": 1 - c}
    prv = {"z": rem(z + NZ - 1 + div(x + NX - 1 + c, NX), NZ), "x": rem(x + NX - 1 + c, NX), "c": 1 - c}
    barrier = pltpu.get_barrier_semaphore()
    near = [nxt, prv] + [{"y": rem(y + q, NY)} for q in range(1, NY)]
    near += [{"z": rem(z + NEAR, NZ)}, {"z": rem(z + NZ - NEAR, NZ)}] + [mate(*to) for to in mates]
    for to in near:
        pl.semaphore_signal(barrier, inc=1, device_id=to, device_id_type=MESH)

    in_pv.wait()
    in_pg.wait()

    def gate_rows(r0, rows):
        for h in range(2):
            lanes = pl.ds(128 * h, 128)
            s = sigmoid(pg[pl.ds(r0, rows), lanes].astype(F32))
            g = (pv[pl.ds(r0, rows), lanes].astype(F32) * s).astype(BF16)
            sg[h, pl.ds(r0, rows), :] = s
            gp[h, pl.ds(r0 + HALO, rows), :] = g.astype(F32)
            yield lanes, g
    for lanes, g in gate_rows(length - HALO, HALO):
        hs[:, lanes] = g

    @pl.loop(0, (length - HALO) // 32)
    def _(i):
        for _ in gate_rows(pl.multiple_of(i * 32, 32), 32):
            pass

    for cp in in_small:
        cp.wait()
    for h in range(2):
        wt[h, 0:taps, :] = taps_b[:, pl.ds(128 * h, 128)].astype(F32)
    gain = [gain_v[pl.ds(128 * h, 128)].reshape(1, 128) for h in range(2)]
    for b in range(blocks):
        rows = pl.ds(128 * b, 128)
        rm[rows, :] = jnp.broadcast_to(mean_v[rows].reshape(1, 128), (128, 128)).T
        rs[rows, :] = jnp.broadcast_to(scale_v[rows].reshape(1, 128), (128, 128)).T
    pl.semaphore_wait(barrier, len(near))
    halo = pltpu.make_async_remote_copy(hs, hr, halo_sem.at[0], halo_sem.at[1], device_id=nxt, device_id_type=MESH)
    halo.start()

    def far(step, k):
        for to in (rem(z + step, NZ), rem(z + NZ - step, NZ)):
            pl.semaphore_signal(far_sem.at[k], inc=1, device_id={"z": to}, device_id_type=MESH)

    far(NEAR, 0)

    in_ow.wait()
    for cp in in_cot:
        cp.wait()
    u = lax.dot_general(cot[...], ow[...], (((1,), (1,)), ((), ())), preferred_element_type=F32)
    for h in range(2):
        us[h, :, :] = u[:, 128 * h:128 * h + 128]

    def conv_rows(h, r0, rows):
        acc = jnp.zeros((rows, 128), F32)
        for k in range(taps):
            acc = acc + wt[h, k:k + 1, :] * gp[h, pl.ds(r0 + (HALO + 1 - taps + k), rows), :]
        cv[h, pl.ds(r0, rows), :] = acc

    def point_rows(r0, rows):
        sl = pl.ds(r0, rows)
        sums = []
        for h in range(2):
            n = (cv[h, sl, :] - rm[sl, :]) * rs[sl, :]
            a = n * gain[h]
            s = sigmoid(a)
            hid[sl, pl.ds(128 * h, 128)] = (a * s).astype(BF16)
            da = us[h, sl, :] * s * (1.0 + a * (1.0 - s))
            d = da * gain[h]
            dan = da * n
            gacc[h, :, :] += dan.reshape(rows // 8, 8, 128).sum(axis=0)
            nm[h, sl, :] = n
            dn[h, sl, :] = d
            sums.append((d, dan * gain[h]))
        s1[sl, :] = sums[0][0] + sums[1][0]
        s2[sl, :] = sums[0][1] + sums[1][1]

    gacc[...] = jnp.zeros_like(gacc)
    @pl.loop(0, 8)
    def _(i):
        conv_rows(rem(i, 2), pl.multiple_of(HALO + div(i, 2) * 88, 8), 88)
    pl.semaphore_wait(far_sem.at[0], 2)
    far(2 * NEAR, 1)

    @pl.loop(0, (length - HALO) // 32)
    def _(i):
        point_rows(pl.multiple_of(HALO + i * 32, 32), 32)

    def row_sums(lo, hi):
        for b in range(lo, hi):
            rows = pl.ds(128 * b, 128)
            ys[b, 0:1, :] = jnp.sum(s1[rows, :].T, axis=0, keepdims=True)
            ys[b, 1:2, :] = jnp.sum(s2[rows, :].T, axis=0, keepdims=True)
        cps = []
        for q in (2, 1, 3):
            cps.append(pltpu.make_async_remote_copy(
                ys.at[pl.ds(lo, hi - lo)], yr.at[y, pl.ds(lo, hi - lo)], y_ss.at[q, min(lo, 1)], y_rs.at[q, min(lo, 1)],
                device_id={"y": rem(y + q, NY)}, device_id_type=MESH))
            cps[-1].start()
        return cps
    y_late = row_sums(1, blocks)

    @pl.loop(0, cot.shape[1] // 256)
    def _(i):
        for e in range(2):
            b = pl.multiple_of(i * 256 + 128 * e, 128)
            cot_t[pl.ds(b, 128), :] = cot[:, pl.ds(b, 128)].T
    halo.wait_recv()
    first_dev = ((z * NX + x) * NC + c) == 0
    for h in range(2):
        got = hr[:, pl.ds(128 * h, 128)].astype(F32)
        gp[h, 0:HALO, :] = jnp.where(first_dev, jnp.zeros_like(got), got)
        conv_rows(h, 0, HALO)
    point_rows(0, HALO)
    y_first = row_sums(0, 1)
    yr[y] = ys[...]
    pl.semaphore_wait(far_sem.at[1], 2)
    far(4 * NEAR, 2)

    rows_c = 64 * 2 * HC
    c_cp = []
    for k in range(CHUNKS):
        w = lax.dot_general(
            cot_t[pl.ds(k * rows_c, rows_c), :], hid[...], (((1,), (0,)), ((), ())), preferred_element_type=F32)
        for e in range(HC):
            for pz in range(2):
                for px in range(NX):
                    for pc in range(NC):
                        r = 64 * (2 * e + pz) + 16 * px + 8 * pc
                        for h in range(2):
                            w32[k, pc, pz, px, e, h, :, :] = w[r:r + 8, 128 * h:128 * h + 128]
        c_cp.append(pltpu.make_async_remote_copy(
            w32.at[k, 1 - c], wc.at[k], c_ss.at[k], c_rs.at[k], device_id={"c": 1 - c}, device_id_type=MESH))
        c_cp[-1].start()

    inv = 1.0 / (NY * pv.shape[1])

    def d_conv(lo, hi):
        for b in range(lo, hi):
            rows = pl.ds(128 * b, 128)
            tot = ((yr[0, b] + yr[1, b]) + (yr[2, b] + yr[3, b])) * inv
            s1[rows, :] = jnp.broadcast_to(tot[0:1, :], (128, 128)).T
            s2[rows, :] = jnp.broadcast_to(tot[1:2, :], (128, 128)).T

        @pl.loop(lo * 4, hi * 4)
        def _(i):
            sl = pl.ds(pl.multiple_of(i * 32, 32), 32)
            for h in range(2):
                dcp[h, sl, :] = rs[sl, :] * (dn[h, sl, :] - s1[sl, :] - nm[h, sl, :] * s2[sl, :])

    def tap_rows(lo, hi, start):
        for h in range(2):
            def step(i, acc):
                acc = list(acc)
                for e in range(4):
                    r0 = pl.multiple_of(i * 32 + 8 * e, 8)
                    d = dcp[h, pl.ds(r0, 8), :]
                    for k in range(taps):
                        acc[k] = acc[k] + d * gp[h, pl.ds(r0 + (HALO + 1 - taps + k), 8), :]
                return tuple(acc)
            init = tuple(jnp.zeros((8, 128), F32) if start else kacc[h, k] for k in range(taps))
            acc = lax.fori_loop(lo * 4, hi * 4, step, init)
            for k in range(taps):
                if start:
                    kacc[h, k] = acc[k]
                else:
                    tp[k // 2, 2 * h + k % 2, :] = jnp.sum(acc[k], axis=0)
    for cp in y_late:
        cp.wait_recv()
    d_conv(1, blocks)
    tap_rows(1, blocks, True)
    for h in range(2):
        tp[taps // 2, 2 * h + taps % 2, :] = jnp.sum(gacc[h], axis=0)
    for cp in y_first:
        cp.wait_recv()
    d_conv(0, 1)
    dhalo = pltpu.make_async_remote_copy(
        dcp.at[:, pl.ds(0, HALO), :], dcp.at[:, pl.ds(length, HALO), :], dhalo_sem.at[0], dhalo_sem.at[1],
        device_id=prv, device_id_type=MESH)
    tap_rows(0, 1, False)
    t_cp = []
    for q, to in enumerate(mates):
        t_cp.append(pltpu.make_async_remote_copy(
            tp.at[(to[0] * NX + to[1]) * NC + to[2]], tr.at[m_me], t_ss.at[q], t_rs.at[q],
            device_id=mate(*to), device_id_type=MESH))
        t_cp[-1].start()
    tr[m_me] = tp[m_me]
    dhalo.start()

    x_cp = []
    for k in range(CHUNKS):
        c_cp[k].wait_recv()
        for pz in range(2):
            @pl.loop(0, NX)
            def _(px):
                v = (w32[k, c, pz, px] + wc[k, pz, px]).reshape(HC, 16, 128)
                xs[k, pz, px] = v.astype(BF16)
        for pz, px, q in wmates:
            x_cp.append(pltpu.make_async_remote_copy(
                xs.at[k, pz, px], xr.at[q, k], x_ss.at[q, k], x_rs.at[q, k],
                device_id=mate(pz, px, c), device_id_type=MESH))
            x_cp[-1].start()

    pl.semaphore_wait(far_sem.at[2], 2)
    for cp in t_cp:
        cp.wait_recv()
    share = ((tr[0] + tr[1]) + (tr[2] + tr[3])) + ((tr[4] + tr[5]) + (tr[6] + tr[7]))
    share = share + (((tr[8] + tr[9]) + (tr[10] + tr[11])) + ((tr[12] + tr[13]) + (tr[14] + tr[15])))
    tf[0] = share

    def z_copy(src, dst, ss, rs_, d):
        return pltpu.make_async_remote_copy(
            src, dst, ss.at[d], rs_.at[d], device_id={"z": rem(z + 2 * d, NZ)}, device_id_type=MESH)

    by_distance = [NH // 2]
    for d in range(NH // 2 - 1, 0, -1):
        by_distance += [d, NH - d]
    for d in by_distance:
        z_copy(tf.at[0], tz.at[zh], tz_ss, tz_rs, d).start()
    tz[zh] = share

    for cp in x_cp:
        cp.wait_recv()
    for k in range(CHUNKS):
        v = (w32[k, c, zp, x] + wc[k, zp, x]).reshape(HC, 16, 128)
        for q in range(2 * NX - 1):
            v = v + xr[q, k].astype(F32)
        zo[pl.ds(k * HC, HC)] = v
        zs[pl.ds(k * HC, HC)] = v.astype(BF16)
    for d in by_distance:
        z_copy(zs.at[rem(zh + d, NH)], zr.at[zh], z_ss, z_rs, d).start()

    last_dev = ((z * NX + x) * NC + c) == NZ * NX * NC - 1
    dhalo.wait_recv()
    for h in range(2):
        got = dcp[h, pl.ds(length, HALO), :]
        dcp[h, pl.ds(length, HALO), :] = jnp.where(last_dev, jnp.zeros_like(got), got)
    for h in range(2):
        @pl.loop(0, length // 64)
        def _(i):
            r0 = pl.multiple_of(i * 64, 64)
            acc = jnp.zeros((64, 128), F32)
            for k in range(taps):
                acc = acc + wt[h, k:k + 1, :] * dcp[h, pl.ds(r0 + (taps - 1 - k), 64), :]
            sl, lanes = pl.ds(r0, 64), pl.ds(128 * h, 128)
            s = sg[h, sl, :]
            vg_o[sl, lanes] = (acc * s).astype(BF16)
            gg_o[sl, lanes] = (acc * pv[sl, lanes].astype(F32) * s * (1.0 - s)).astype(BF16)

    for d in range(1, NH):
        z_copy(tf.at[0], tz.at[zh], tz_ss, tz_rs, d).wait_recv()
    parts = [tz[i] for i in range(NH)]
    while len(parts) > 1:
        parts = [a + b for a, b in zip(parts[::2], parts[1::2])]
    total = parts[0]
    tf[1] = total
    f_cp = []
    for q, to in enumerate(mates):
        f_cp.append(pltpu.make_async_remote_copy(
            tf.at[1], tacc.at[m_me], tf_ss.at[q], tf_rs.at[q], device_id=mate(*to), device_id_type=MESH))
        f_cp[-1].start()
    tacc[m_me] = total

    for d in range(1, NH):
        z_copy(zs.at[0], zr.at[zh], z_ss, z_rs, d).wait_recv()
    zr[zh] = jnp.zeros((16, 128), BF16)
    parts = [zo[zh]] + [zr[i].astype(F32) for i in range(NH)]
    while len(parts) > 1:
        parts = [a + b for a, b in zip(parts[::2], parts[1::2])] + parts[len(parts) // 2 * 2:]
    for h in range(2):
        wg_o[:, pl.ds(128 * h, 128)] = parts[0][8 * h:8 * h + 8, :]
    for cp in f_cp:
        cp.wait_recv()
    for k in range(taps + 1):
        for h in range(2):
            row = tacc[k // 2, 2 * h + k % 2:2 * h + k % 2 + 1, :]
            if k < taps:
                tg_o[k:k + 1, pl.ds(128 * h, 128)] = row
            else:
                gn_o[pl.ds(128 * h, 128)] = row.reshape(128)

    halo.wait_send()
    dhalo.wait_send()
    for cp in y_late + y_first + c_cp + x_cp + t_cp + f_cp:
        cp.wait_send()
    for d in range(1, NH):
        z_copy(tf.at[0], tz.at[zh], tz_ss, tz_rs, d).wait_send()
        z_copy(zs.at[0], zr.at[zh], z_ss, z_rs, d).wait_send()


def out_kernel(*refs):
    n = len(refs) // 2
    sems = refs[-1]
    cps = [pltpu.make_async_copy(refs[k], refs[n + k], sems.at[k]) for k in range(n)]
    for cp in cps:
        cp.start()
    for cp in cps:
        cp.wait()


def shards(pv, pg, cot, ow, taps, gain, mean, scale):
    length, ch = pv.shape
    d = cot.shape[1]
    blocks = length // 128
    V, D = pltpu.VMEM, pltpu.SemaphoreType.DMA
    any_spec, vmem = pl.BlockSpec(memory_space=pl.ANY), pl.BlockSpec(memory_space=pltpu.VMEM)
    scratch = [
        V((length, ch), BF16), V((length, ch), BF16), V((length, d), BF16), V((ch, d), BF16),
        V(taps.shape, BF16), V((ch,), F32), V((length,), F32), V((length,), F32),
        V((HALO, ch), BF16), V((HALO, ch), BF16),
        V((2, length + HALO, 128), F32), V((2, length, 128), F32), V((2, length, 128), F32),
        V((2, length, 128), F32), V((2, length, 128), F32), V((2, length, 128), F32),
        V((length, ch), BF16), V((2, length + HALO, 128), F32),
        V((length, 128), F32), V((length, 128), F32), V((length, 128), F32), V((length, 128), F32),
        V((2, 32, 128), F32), V((2, 8, 128), F32),
        V((d, length), BF16),
        V((blocks, 2, 128), F32), V((NY, blocks, 2, 128), F32),
        V((2, 32, 8, 128), F32),
        V((16, 4, 128), F32), V((16, 4, 128), F32), V((16, 4, 128), F32), V((NH, 4, 128), F32), V((2, 4, 128), F32),
        V((CHUNKS, NC, 2, NX, HC, 2, 8, 128), F32), V((CHUNKS, 2, NX, HC, 2, 8, 128), F32),
        V((CHUNKS, 2, NX, HC, 16, 128), BF16), V((2 * NX - 1, CHUNKS, HC, 16, 128), BF16),
        V((NH, 16, 128), BF16), V((NH, 16, 128), F32), V((NH, 16, 128), BF16),
        D((10,)), D((2,)), D((2,)), D((NY, 2)), D((NY, 2)), D((15,)), D((15,)), D((NH,)), D((NH,)), D((15,)), D((15,)),
        D((CHUNKS,)), D((CHUNKS,)), D((2 * NX - 1, CHUNKS)), D((2 * NX - 1, CHUNKS)), D((NH,)), D((NH,)),
        pltpu.SemaphoreType.REGULAR((3,)),
    ]
    outs = (((length, ch), BF16), ((length, ch), BF16), ((8, ch), F32), (taps.shape, F32), ((ch,), F32))
    res = pl.pallas_call(
        main_kernel,
        out_shape=tuple(V(s, t) for s, t in outs),
        in_specs=[any_spec] * 8,
        out_specs=(vmem,) * 5,
        scratch_shapes=scratch,
        name="conv_back",
        compiler_params=pltpu.CompilerParams(collective_id=0, has_side_effects=True, vmem_limit_bytes=56 * 2**20),
    )(pv, pg, cot, ow, taps, gain, mean, scale)
    return pl.pallas_call(
        out_kernel,
        out_shape=tuple(jax.ShapeDtypeStruct(s, t) for s, t in outs),
        in_specs=[vmem] * 5,
        out_specs=(any_spec,) * 5,
        scratch_shapes=[D((5,))],
        name="write_out",
    )(*(pltpu.with_memory_space_constraint(r, pltpu.VMEM) for r in res))


def solution(mesh):
    split = Mesh(mesh.devices.reshape(NZ, NX, NC, mesh.shape["tp"]), ("z", "x", "c", "y"))
    placed = (P(SP, "y"), P(SP, "y"), P(SP, None), P("y", None), P(None, "y"), P("y"), P(SP), P(SP))
    return jax.shard_map(
        shards, mesh=split, in_specs=placed,
        out_specs=(P(SP, "y"), P(SP, "y"), P(SP, "y"), P(None, "y"), P("y")), check_vma=False,
    )
```

time: 77.9 us -> 56.8 us (0.73)
  the two profiles are of different devices: /device:TPU:24 before, /device:TPU:1 now
where the time goes in v2:
time: 56.8 us; the launch traced here: 56.6 us
  Pallas kernels  56 us (99%)
  between operations  0.64 us (1%)
    pallas_call x1, Pallas kernels, shards(): pl.pallas_call(main_kernel, out_shape=tuple((V(s, t) for s, t in outs)),...  55.2 us

profile of v2, /device:TPU:1, one launch (start us, length us, event | category | flops | bytes accessed | tf_op | source)
XLA Modules:
  0.0 56.6 jit_solution(8750125405130324363)
XLA Ops:
  0.6 55.2 %conv_back.1 = (bf16[384,256]{1,0:T(8,128)(2,1)S(1)}, bf16[384,256]{1,0:T(8,128)(2,1)S(1)}, f32[8,256]{1,0:T(8,128)S(1)}, f32[31,256]{1,0:T(8,128)S(1)}, f32[256]{0:T(256)S(1)}) custom-call(bf16[384,256]{1,0:T(8,128)(2,1)} %pv_h.1, bf16[384,256]{1,0:T(8,128)(2,1)} %pg_h.1, bf16[384,2048]{1,0:T(8,128)(2,1)} %cot_h.1, bf16[256,2048]{1,0:T(8,128)(2,1)} %ow_h.1, ...), custom_call_target="tpu_custom_call" | custom-call | tf_op jit(solution)/shard_map/conv_back/pallas_call | solution.py:398
  55.8 0.8 %write_out.1 = (bf16[384,256]{1,0:T(8,128)(2,1)}, bf16[384,256]{1,0:T(8,128)(2,1)}, f32[8,256]{1,0:T(8,128)}, f32[31,256]{1,0:T(8,128)}, f32[256]{0:T(256)}) custom-call(bf16[384,256]{1,0:T(8,128)(2,1)S(1)} %get-tuple-element.10.refs_0_, bf16[384,256]{1,0:T(8,128)(2,1)S(1)} %get-tuple-element.11.refs_1_, f32[8,256]{1,0:T(8,128)S(1)} %get-tuple-element.12.refs_2_, ...), custom_call_target="tpu_custom_call" | custom-call | tf_op jit(solution)/shard_map/write_out/pallas_call | solution.py:407

commit v3 on v2

--- a/solution.py
+++ b/solution.py
@@ -38,7 +38,7 @@
     z, x, c, y = (lax.axis_index(a) for a in ("z", "x", "c", "y"))
     rem, div = lax.rem, lax.div
     zh, zp = div(z, 2), rem(z, 2)
-    m_me = (zp * NX + x) * NC + c
+    g_me = zp * NX + x
 
     def copy_in(src, dst, k):
         cp = pltpu.make_async_copy(src, dst, in_sem.at[k])
@@ -53,12 +53,12 @@
     part = length // 3
     in_cot = [copy_in(cot_h.at[pl.ds(part * k, part), :], cot.at[pl.ds(part * k, part), :], 7 + k) for k in range(3)]
 
-    mates = []
+    steps = [(dx, dz, dc) for dx in (2, 1, 3, 0) for dz in range(2) for dc in range(NC) if dx or dz or dc]
+    mates = [(rem(zp + dz, 2), rem(x + dx, NX), rem(c + dc, NC)) for dx, dz, dc in steps]
+    owners = []
     for dx in (2, 1, 3, 0):
-        for dz in range(2):
-            for dc in range(NC):
-                if dx or dz or dc:
-                    mates.append((rem(zp + dz, 2), rem(x + dx, NX), rem(c + dc, NC)))
+        for dz in (1, 0):
+            owners.append((rem(zp + dz, 2), rem(x + dx, NX), dz * NX + dx))
     wmates = []
     for dx in (2, 1, 3, 0):
         for dz in range(2):
@@ -170,11 +170,12 @@
         return cps
     y_late = row_sums(1, blocks)
 
-    @pl.loop(0, cot.shape[1] // 256)
+    @pl.loop(0, NH // 2)
     def _(i):
         for e in range(2):
-            b = pl.multiple_of(i * 256 + 128 * e, 128)
-            cot_t[pl.ds(b, 128), :] = cot[:, pl.ds(b, 128)].T
+            r = 2 * i + e
+            lanes = pl.ds(pl.multiple_of(rem(zh + r, NH) * 128, 128), 128)
+            cot_t[pl.ds(pl.multiple_of(r * 128, 128), 128), :] = cot[:, lanes].T
     halo.wait_recv()
     first_dev = ((z * NX + x) * NC + c) == 0
     for h in range(2):
@@ -184,14 +185,11 @@
     point_rows(0, HALO)
     y_first = row_sums(0, 1)
     yr[y] = ys[...]
-    pl.semaphore_wait(far_sem.at[1], 2)
-    far(4 * NEAR, 2)
-
     rows_c = 64 * 2 * HC
     c_cp = []
     for k in range(CHUNKS):
         w = lax.dot_general(
-            cot_t[pl.ds(k * rows_c, rows_c), :], hid[...], (((1,), (0,)), ((), ())), preferred_element_type=F32)
+            cot_t[pl.ds((k + 1) % CHUNKS * rows_c, rows_c), :], hid[...], (((1,), (0,)), ((), ())), preferred_element_type=F32)
         for e in range(HC):
             for pz in range(2):
                 for px in range(NX):
@@ -202,6 +200,25 @@
         c_cp.append(pltpu.make_async_remote_copy(
             w32.at[k, 1 - c], wc.at[k], c_ss.at[k], c_rs.at[k], device_id={"c": 1 - c}, device_id_type=MESH))
         c_cp[-1].start()
+    pl.semaphore_wait(far_sem.at[1], 2)
+    far(4 * NEAR, 2)
+
+    x_cp = [[], []]
+
+    def x_phase(p):
+        for k in (2 * p, 2 * p + 1):
+            c_cp[k].wait_recv()
+            for pz in range(2):
+                @pl.loop(0, NX)
+                def _(px):
+                    v = (w32[k, c, pz, px] + wc[k, pz, px]).reshape(HC, 16, 128)
+                    xs[p, pz, px, k % 2 * HC:(k % 2 + 1) * HC] = v.astype(BF16)
+        for pz, px, q in wmates:
+            x_cp[p].append(pltpu.make_async_remote_copy(
+                xs.at[p, pz, px], xr.at[q, p], x_ss.at[q, p], x_rs.at[q, p],
+                device_id=mate(pz, px, c), device_id_type=MESH))
+            x_cp[p][-1].start()
+    x_phase(0)
 
     inv = 1.0 / (NY * pv.shape[1])
 
@@ -234,13 +251,13 @@
                 if start:
                     kacc[h, k] = acc[k]
                 else:
-                    tp[k // 2, 2 * h + k % 2, :] = jnp.sum(acc[k], axis=0)
+                    tp[k // 4, 4 * h + k % 4, :] = jnp.sum(acc[k], axis=0)
     for cp in y_late:
         cp.wait_recv()
     d_conv(1, blocks)
     tap_rows(1, blocks, True)
     for h in range(2):
-        tp[taps // 2, 2 * h + taps % 2, :] = jnp.sum(gacc[h], axis=0)
+        tp[taps // 4, 4 * h + taps % 4, :] = jnp.sum(gacc[h], axis=0)
     for cp in y_first:
         cp.wait_recv()
     d_conv(0, 1)
@@ -249,34 +266,33 @@
         device_id=prv, device_id_type=MESH)
     tap_rows(0, 1, False)
     t_cp = []
-    for q, to in enumerate(mates):
+    for pz, px, q in owners:
         t_cp.append(pltpu.make_async_remote_copy(
-            tp.at[(to[0] * NX + to[1]) * NC + to[2]], tr.at[m_me], t_ss.at[q], t_rs.at[q],
-            device_id=mate(*to), device_id_type=MESH))
+            tp.at[pz * NX + px], tr.at[c, g_me], t_ss.at[q], t_rs.at[c, q], device_id=mate(pz, px, 1), device_id_type=MESH))
+    for cp in t_cp[:-1]:
+        cp.start()
+
+    @pl.when(c == 0)
+    def _():
         t_cp[-1].start()
-    tr[m_me] = tp[m_me]
+
+    @pl.when(c == 1)
+    def _():
+        tr[c, g_me] = tp[g_me]
     dhalo.start()
-
-    x_cp = []
-    for k in range(CHUNKS):
-        c_cp[k].wait_recv()
-        for pz in range(2):
-            @pl.loop(0, NX)
-            def _(px):
-                v = (w32[k, c, pz, px] + wc[k, pz, px]).reshape(HC, 16, 128)
-                xs[k, pz, px] = v.astype(BF16)
-        for pz, px, q in wmates:
-            x_cp.append(pltpu.make_async_remote_copy(
-                xs.at[k, pz, px], xr.at[q, k], x_ss.at[q, k], x_rs.at[q, k],
-                device_id=mate(pz, px, c), device_id_type=MESH))
-            x_cp[-1].start()
-
-    pl.semaphore_wait(far_sem.at[2], 2)
-    for cp in t_cp:
-        cp.wait_recv()
-    share = ((tr[0] + tr[1]) + (tr[2] + tr[3])) + ((tr[4] + tr[5]) + (tr[6] + tr[7]))
-    share = share + (((tr[8] + tr[9]) + (tr[10] + tr[11])) + ((tr[12] + tr[13]) + (tr[14] + tr[15])))
-    tf[0] = share
+    x_phase(1)
+
+    def d_gated(h, r0, rows):
+        acc = jnp.zeros((rows, 128), F32)
+        for k in range(taps):
+            acc = acc + wt[h, k:k + 1, :] * dcp[h, pl.ds(r0 + (taps - 1 - k), rows), :]
+        sl, lanes = pl.ds(r0, rows), pl.ds(128 * h, 128)
+        s = sg[h, sl, :]
+        vg_o[sl, lanes] = (acc * s).astype(BF16)
+        gg_o[sl, lanes] = (acc * pv[sl, lanes].astype(F32) * s * (1.0 - s)).astype(BF16)
+    @pl.loop(0, 2 * ((length - HALO) // 32))
+    def _(i):
+        d_gated(rem(i, 2), pl.multiple_of(div(i, 2) * 32, 32), 32)
 
     def z_copy(src, dst, ss, rs_, d):
         return pltpu.make_async_remote_copy(
@@ -285,77 +301,103 @@
     by_distance = [NH // 2]
     for d in range(NH // 2 - 1, 0, -1):
         by_distance += [d, NH - d]
-    for d in by_distance:
-        z_copy(tf.at[0], tz.at[zh], tz_ss, tz_rs, d).start()
-    tz[zh] = share
-
-    for cp in x_cp:
-        cp.wait_recv()
-    for k in range(CHUNKS):
-        v = (w32[k, c, zp, x] + wc[k, zp, x]).reshape(HC, 16, 128)
-        for q in range(2 * NX - 1):
-            v = v + xr[q, k].astype(F32)
-        zo[pl.ds(k * HC, HC)] = v
-        zs[pl.ds(k * HC, HC)] = v.astype(BF16)
-    for d in by_distance:
-        z_copy(zs.at[rem(zh + d, NH)], zr.at[zh], z_ss, z_rs, d).start()
-
+
+    def tree(parts):
+        while len(parts) > 1:
+            parts = [a + b for a, b in zip(parts[::2], parts[1::2])] + parts[len(parts) // 2 * 2:]
+        return parts[0]
+
+    def z_phase(p):
+        for cp in x_cp[p]:
+            cp.wait_recv()
+        for k in (2 * p, 2 * p + 1):
+            v = (w32[k, c, zp, x] + wc[k, zp, x]).reshape(HC, 16, 128)
+            for q in range(2 * NX - 1):
+                v = v + xr[q, p, k % 2 * HC:(k % 2 + 1) * HC].astype(F32)
+            r0 = (k + 1) % CHUNKS * HC
+            if r0 == 0:
+                zo[...] = v[0]
+            zs[r0:r0 + HC] = v.astype(BF16)
+        for d in by_distance:
+            if (HC <= d < 3 * HC) == (p == 0):
+                z_copy(zs.at[d], zr.at[d], z_ss, z_rs, d).start()
+    pl.semaphore_wait(far_sem.at[2], 2)
+
+
+    @pl.when(c == 1)
+    def _():
+        for pz, px, q in owners:
+            for pc in range(NC):
+                if q or pc == 0:
+                    pltpu.make_async_remote_copy(
+                        tp.at[0], tr.at[pc, 0], t_ss.at[q], t_rs.at[pc, q], device_id=mate(pz, px, 1), device_id_type=MESH
+                    ).wait_recv()
+        share = tree([tr[pc, g] for pc in range(NC) for g in range(2 * NX)])
+        tf[0] = share
+        for d in by_distance:
+            z_copy(tf.at[0], tz.at[zh], tz_ss, tz_rs, d).start()
+        tz[zh] = share
+    z_phase(0)
+    z_phase(1)
     last_dev = ((z * NX + x) * NC + c) == NZ * NX * NC - 1
     dhalo.wait_recv()
     for h in range(2):
         got = dcp[h, pl.ds(length, HALO), :]
         dcp[h, pl.ds(length, HALO), :] = jnp.where(last_dev, jnp.zeros_like(got), got)
-    for h in range(2):
-        @pl.loop(0, length // 64)
-        def _(i):
-            r0 = pl.multiple_of(i * 64, 64)
-            acc = jnp.zeros((64, 128), F32)
-            for k in range(taps):
-                acc = acc + wt[h, k:k + 1, :] * dcp[h, pl.ds(r0 + (taps - 1 - k), 64), :]
-            sl, lanes = pl.ds(r0, 64), pl.ds(128 * h, 128)
-            s = sg[h, sl, :]
-            vg_o[sl, lanes] = (acc * s).astype(BF16)
-            gg_o[sl, lanes] = (acc * pv[sl, lanes].astype(F32) * s * (1.0 - s)).astype(BF16)
+        d_gated(h, length - HALO, HALO)
+
+    halo.wait_send()
+    dhalo.wait_send()
+    for cp in y_late + y_first + c_cp + x_cp[0] + x_cp[1] + t_cp[:-1]:
+        cp.wait_send()
+
+    @pl.when(c == 0)
+    def _():
+        t_cp[-1].wait_send()
+
+    def f_copy(q, to):
+        return pltpu.make_async_remote_copy(
+            tf.at[1], tacc.at[g_me], tf_ss.at[q], tf_rs.at[q], device_id=mate(*to), device_id_type=MESH)
+
+    @pl.when(c == 1)
+    def _():
+        for d in range(1, NH):
+            z_copy(tf.at[0], tz.at[zh], tz_ss, tz_rs, d).wait_recv()
+        total = tree([tz[i] for i in range(NH)])
+        tf[1] = total
+        for q, to in enumerate(mates):
+            f_copy(q, to).start()
+        tacc[g_me] = total
 
     for d in range(1, NH):
-        z_copy(tf.at[0], tz.at[zh], tz_ss, tz_rs, d).wait_recv()
-    parts = [tz[i] for i in range(NH)]
-    while len(parts) > 1:
-        parts = [a + b for a, b in zip(parts[::2], parts[1::2])]
-    total = parts[0]
-    tf[1] = total
-    f_cp = []
-    for q, to in enumerate(mates):
-        f_cp.append(pltpu.make_async_remote_copy(
-            tf.at[1], tacc.at[m_me], tf_ss.at[q], tf_rs.at[q], device_id=mate(*to), device_id_type=MESH))
-        f_cp[-1].start()
-    tacc[m_me] = total
-
+        z_copy(zs.at[d], zr.at[d], z_ss, z_rs, d).wait_recv()
+    wsum = tree([zo[...]] + [zr[i].astype(F32) for i in range(1, NH)])
+    for h in range(2):
+        wg_o[:, pl.ds(128 * h, 128)] = wsum[8 * h:8 * h + 8, :]
     for d in range(1, NH):
-        z_copy(zs.at[0], zr.at[zh], z_ss, z_rs, d).wait_recv()
-    zr[zh] = jnp.zeros((16, 128), BF16)
-    parts = [zo[zh]] + [zr[i].astype(F32) for i in range(NH)]
-    while len(parts) > 1:
-        parts = [a + b for a, b in zip(parts[::2], parts[1::2])] + parts[len(parts) // 2 * 2:]
-    for h in range(2):
-        wg_o[:, pl.ds(128 * h, 128)] = parts[0][8 * h:8 * h + 8, :]
-    for cp in f_cp:
-        cp.wait_recv()
+        z_copy(zs.at[d], zr.at[d], z_ss, z_rs, d).wait_send()
+
+    @pl.when(c == 1)
+    def _():
+        for d in range(1, NH):
+            z_copy(tf.at[0], tz.at[zh], tz_ss, tz_rs, d).wait_send()
+
+    for q, (dx, dz, dc) in enumerate(steps):
+        @pl.when(rem(c + dc, 2) == 1)
+        def _():
+            f_copy(q, mates[q]).wait_recv()
     for k in range(taps + 1):
         for h in range(2):
-            row = tacc[k // 2, 2 * h + k % 2:2 * h + k % 2 + 1, :]
+            row = tacc[k // 4, 4 * h + k % 4:4 * h + k % 4 + 1, :]
             if k < taps:
                 tg_o[k:k + 1, pl.ds(128 * h, 128)] = row
             else:
                 gn_o[pl.ds(128 * h, 128)] = row.reshape(128)
 
-    halo.wait_send()
-    dhalo.wait_send()
-    for cp in y_late + y_first + c_cp + x_cp + t_cp + f_cp:
-        cp.wait_send()
-    for d in range(1, NH):
-        z_copy(tf.at[0], tz.at[zh], tz_ss, tz_rs, d).wait_send()
-        z_copy(zs.at[0], zr.at[zh], z_ss, z_rs, d).wait_send()
+    @pl.when(c == 1)
+    def _():
+        for q, to in enumerate(mates):
+            f_copy(q, to).wait_send()
 
 
 def out_kernel(*refs):
@@ -386,12 +428,12 @@
         V((d, length), BF16),
         V((blocks, 2, 128), F32), V((NY, blocks, 2, 128), F32),
         V((2, 32, 8, 128), F32),
-        V((16, 4, 128), F32), V((16, 4, 128), F32), V((16, 4, 128), F32), V((NH, 4, 128), F32), V((2, 4, 128), F32),
+        V((8, 8, 128), F32), V((8, 8, 128), F32), V((NC, 8, 8, 128), F32), V((NH, 8, 128), F32), V((2, 8, 128), F32),
         V((CHUNKS, NC, 2, NX, HC, 2, 8, 128), F32), V((CHUNKS, 2, NX, HC, 2, 8, 128), F32),
-        V((CHUNKS, 2, NX, HC, 16, 128), BF16), V((2 * NX - 1, CHUNKS, HC, 16, 128), BF16),
-        V((NH, 16, 128), BF16), V((NH, 16, 128), F32), V((NH, 16, 128), BF16),
-        D((10,)), D((2,)), D((2,)), D((NY, 2)), D((NY, 2)), D((15,)), D((15,)), D((NH,)), D((NH,)), D((15,)), D((15,)),
-        D((CHUNKS,)), D((CHUNKS,)), D((2 * NX - 1, CHUNKS)), D((2 * NX - 1, CHUNKS)), D((NH,)), D((NH,)),
+        V((2, 2, NX, NH // 2, 16, 128), BF16), V((2 * NX - 1, 2, NH // 2, 16, 128), BF16),
+        V((NH, 16, 128), BF16), V((16, 128), F32), V((NH, 16, 128), BF16),
+        D((10,)), D((2,)), D((2,)), D((NY, 2)), D((NY, 2)), D((8,)), D((NC, 8)), D((NH,)), D((NH,)), D((15,)), D((15,)),
+        D((CHUNKS,)), D((CHUNKS,)), D((2 * NX - 1, 2)), D((2 * NX - 1, 2)), D((NH,)), D((NH,)),
         pltpu.SemaphoreType.REGULAR((3,)),
     ]
     outs = (((length, ch), BF16), ((length, ch), BF16), ((8, ch), F32), (taps.shape, F32), ((ch,), F32))

time: 56.8 us -> 53.9 us (0.949)
  Pallas kernels: 56 us -> 53.1 us
    pallas_call x1, Pallas kernels: 55.2 us -> 52.3 us  [shards(): pl.pallas_call(main_kernel, out_shape=tuple((V(s, t) for s, t in outs)),...]
where the time goes in v3:
time: 53.9 us; the launch traced here: 53.8 us
  Pallas kernels  53.1 us (99%)
  between operations  0.64 us (1%)
    pallas_call x1, Pallas kernels, shards(): pl.pallas_call(main_kernel, out_shape=tuple((V(s, t) for s, t in outs)),...  52.3 us

profile of v3, /device:TPU:1, one launch (start us, length us, event | category | flops | bytes accessed | tf_op | source)
XLA Modules:
  0.0 53.8 jit_solution(7977128248230590041)
XLA Ops:
  0.6 52.3 %conv_back.1 = (bf16[384,256]{1,0:T(8,128)(2,1)S(1)}, bf16[384,256]{1,0:T(8,128)(2,1)S(1)}, f32[8,256]{1,0:T(8,128)S(1)}, f32[31,256]{1,0:T(8,128)S(1)}, f32[256]{0:T(256)S(1)}) custom-call(bf16[384,256]{1,0:T(8,128)(2,1)} %pv_h.1, bf16[384,256]{1,0:T(8,128)(2,1)} %pg_h.1, bf16[384,2048]{1,0:T(8,128)(2,1)} %cot_h.1, bf16[256,2048]{1,0:T(8,128)(2,1)} %ow_h.1, ...), custom_call_target="tpu_custom_call" | custom-call | tf_op jit(solution)/shard_map/conv_back/pallas_call | solution.py:440
  53.0 0.8 %write_out.1 = (bf16[384,256]{1,0:T(8,128)(2,1)}, bf16[384,256]{1,0:T(8,128)(2,1)}, f32[8,256]{1,0:T(8,128)}, f32[31,256]{1,0:T(8,128)}, f32[256]{0:T(256)}) custom-call(bf16[384,256]{1,0:T(8,128)(2,1)S(1)} %get-tuple-element.10.refs_0_, bf16[384,256]{1,0:T(8,128)(2,1)S(1)} %get-tuple-element.11.refs_1_, f32[8,256]{1,0:T(8,128)S(1)} %get-tuple-element.12.refs_2_, ...), custom_call_target="tpu_custom_call" | custom-call | tf_op jit(solution)/shard_map/write_out/pallas_call | solution.py:449

commit v4 on v3

v4 whole, which is shorter than its diff:
```python
import functools

import jax
import jax.numpy as jnp
from jax import lax
from jax.experimental import pallas as pl
from jax.experimental.pallas import tpu as pltpu
from jax.sharding import Mesh
from jax.sharding import PartitionSpec as P

MESH = pl.DeviceIdType.MESH
SP = ("z", "x", "c")
NZ, NX, NC, NY = 32, 4, 2, 4
F32, BF16 = jnp.float32, jnp.bfloat16
HALO = 32
NH = NZ // 2
CHUNKS = 4
HC = NH // CHUNKS


def sigmoid(v):
    return 1.0 / (1.0 + jnp.exp(-v))


def main_kernel(
    pv_h, pg_h, cot_h, ow_h, taps_h, gain_h, mean_h, scale_h,
    vg_o, gg_o, wg_o, tg_o, gn_o,
    pvg, cot, ow, taps_b, gain_v, mean_v, scale_v,
    hs, hr, gp, sg, us, cv, nm, dn, hid, dcp, rm, rs, s1, s2, wt, gacc,
    cot_t, ys, yr, ys0, yr0, kacc, tacc, tp, tr, tz, tf, w32, wc, xs, xr, zs, zr,
    in_sem, halo_sem, dhalo_sem, y_ss, y_rs, t_ss, t_rs, tz_ss, tz_rs, tf_ss, tf_rs,
    c_ss, c_rs, x_ss, x_rs, z_ss, z_rs, far_sem,
):
    length = pvg.shape[1]
    taps = taps_b.shape[0]
    blocks = length // 128
    z, x, c, y = (lax.axis_index(a) for a in ("z", "x", "c", "y"))
    rem, div = lax.rem, lax.div
    zh, zp = div(z, 2), rem(z, 2)
    g_me, g_sum = zp * NX + x, (1 - zp) * NX + x

    def copy_in(src, dst, k):
        cp = pltpu.make_async_copy(src, dst, in_sem.at[k])
        cp.start()
        return cp

    def wait_for(ref, sem):
        pltpu.make_async_copy(ref, ref, sem).wait()

    copy_in(pv_h, pvg.at[0], 0)
    copy_in(pg_h, pvg.at[1], 0)
    in_small = [copy_in(s, d, 1 + k) for k, (s, d) in enumerate(
        ((taps_h, taps_b), (gain_h, gain_v), (mean_h, mean_v), (scale_h, scale_v)))]
    rows_w = cot.shape[0] // 6
    for src, dst, sem in ((ow_h, ow, 5), (cot_h, cot, 6)):
        for k in range(dst.shape[0] // rows_w):
            rows = pl.ds(rows_w * k, rows_w)
            copy_in(src.at[rows, :], dst.at[rows, :], sem)

    steps = [(dx, dz, dc) for dx in (2, 1, 3, 0) for dz in range(2) for dc in range(NC) if dx or dz or dc]
    mates = [(rem(zp + dz, 2), rem(x + dx, NX), rem(c + dc, NC)) for dx, dz, dc in steps]
    owners = []
    for dx in (2, 1, 3, 0):
        for dz in (1, 0):
            owners.append((rem(zp + dz, 2), rem(x + dx, NX), dz * NX + dx))
    wmates = []
    for dx in (2, 1, 3, 0):
        for dz in range(2):
            if dx or dz:
                wmates.append((rem(zp + dz, 2), rem(x + dx, NX), dz * NX + dx - 1))

    def mate(pz, px, pc):
        return {"z": 2 * zh + pz, "x": px, "c": pc}

    nxt = {"z": rem(z + div(x * NC + c + 1, NX * NC), NZ), "x": rem(x + c, NX), "c": 1 - c}
    prv = {"z": rem(z + NZ - 1 + div(x + NX - 1 + c, NX), NZ), "x": rem(x + NX - 1 + c, NX), "c": 1 - c}
    barrier = pltpu.get_barrier_semaphore()

    def along(axis, size, step):
        me = lax.axis_index(axis)
        return [{axis: rem(me + step, size)}, {axis: rem(me + size - step, size)}]

    core, x1, y1, z1, z2 = [{"c": 1 - c}], along("x", NX, 1), along("y", NY, 1), along("z", NZ, 1), along("z", NZ, 2)
    entry = z2 + [prv, nxt] + x1 + y1 + along("y", NY, 2)[:1] + z1 + core
    for to in entry:
        pl.semaphore_signal(barrier, inc=1, device_id=to, device_id_type=MESH)

    stages = [z2 + core + x1 + y1 + z1, along("z", NZ, 4) + core + along("x", NX, 2)[:1], along("z", NZ, 8)]

    def tell(k):
        for to in stages[k]:
            pl.semaphore_signal(far_sem.at[k], inc=1, device_id=to, device_id_type=MESH)

    def heard(k):
        pl.semaphore_wait(far_sem.at[k], len(stages[k]))

    gacc[...] = jnp.zeros_like(gacc)
    for part in (s1, s2):
        part[0:HALO, :] = jnp.zeros((HALO, 128), F32)

    wait_for(pvg, in_sem.at[0])

    def gate_rows(r0, rows):
        for h in range(2):
            lanes = pl.ds(128 * h, 128)
            s = sigmoid(pvg[1, pl.ds(r0, rows), lanes].astype(F32))
            g = (pvg[0, pl.ds(r0, rows), lanes].astype(F32) * s).astype(BF16)
            sg[h, pl.ds(r0, rows), :] = s
            gp[h, pl.ds(r0 + HALO, rows), :] = g.astype(F32)
            yield lanes, g
    for lanes, g in gate_rows(length - HALO, HALO):
        hs[:, lanes] = g

    @pl.loop(0, (length - HALO) // 32)
    def _(i):
        for _ in gate_rows(pl.multiple_of(i * 32, 32), 32):
            pass

    for cp in in_small:
        cp.wait()
    for h in range(2):
        wt[h, 0:taps, :] = taps_b[:, pl.ds(128 * h, 128)].astype(F32)
    gain = [gain_v[pl.ds(128 * h, 128)].reshape(1, 128) for h in range(2)]
    for b in range(blocks):
        rows = pl.ds(128 * b, 128)
        rm[rows, :] = jnp.broadcast_to(mean_v[rows].reshape(1, 128), (128, 128)).T
        rs[rows, :] = jnp.broadcast_to(scale_v[rows].reshape(1, 128), (128, 128)).T
    pl.semaphore_wait(barrier, len(entry))
    halo = pltpu.make_async_remote_copy(hs, hr, halo_sem.at[0], halo_sem.at[1], device_id=nxt, device_id_type=MESH)
    halo.start()
    tell(0)

    def conv_rows(h, r0, rows):
        acc = jnp.zeros((rows, 128), F32)
        for k in range(taps):
            acc = acc + wt[h, k:k + 1, :] * gp[h, pl.ds(r0 + (HALO + 1 - taps + k), rows), :]
        cv[h, pl.ds(r0, rows), :] = acc

    def point_rows(r0, rows):
        sl = pl.ds(r0, rows)
        sums = []
        for h in range(2):
            n = (cv[h, sl, :] - rm[sl, :]) * rs[sl, :]
            a = n * gain[h]
            s = sigmoid(a)
            hid[sl, pl.ds(128 * h, 128)] = (a * s).astype(BF16)
            da = us[h, sl, :] * s * (1.0 + a * (1.0 - s))
            d = da * gain[h]
            dan = da * n
            gacc[h, :, :] += dan.reshape(rows // 8, 8, 128).sum(axis=0)
            nm[h, sl, :] = n
            dn[h, sl, :] = d
            sums.append((d, dan * gain[h]))
        s1[sl, :] = sums[0][0] + sums[1][0]
        s2[sl, :] = sums[0][1] + sums[1][1]
    @pl.loop(0, 8)
    def _(i):
        conv_rows(rem(i, 2), pl.multiple_of(HALO + div(i, 2) * 88, 8), 88)
    wait_for(ow, in_sem.at[5])
    wait_for(cot, in_sem.at[6])
    u = lax.dot_general(cot[...], ow[...], (((1,), (1,)), ((), ())), preferred_element_type=F32)
    for h in range(2):
        us[h, :, :] = u[:, 128 * h:128 * h + 128]
    @pl.loop(0, (length - HALO) // 32)
    def _(i):
        point_rows(pl.multiple_of(HALO + i * 32, 32), 32)

    def row_sums(lo, hi, part, ys, yr):
        for b in range(lo, hi):
            rows = pl.ds(128 * b, 128)
            ys[b, 0:1, :] = jnp.sum(s1[rows, :].T, axis=0, keepdims=True)
            ys[b, 1:2, :] = jnp.sum(s2[rows, :].T, axis=0, keepdims=True)
        cps = []
        for q in (2, 1, 3):
            cps.append(pltpu.make_async_remote_copy(
                ys, yr.at[y], y_ss.at[part], y_rs.at[part], device_id={"y": rem(y + q, NY)}, device_id_type=MESH))
            cps[-1].start()
        return cps
    y_late = row_sums(0, blocks, 0, ys, yr)
    yr[y] = ys[...]
    heard(0)
    tell(1)

    @pl.loop(0, NH // 2)
    def _(i):
        for e in range(2):
            r = 2 * i + e
            lanes = pl.ds(pl.multiple_of(rem(zh + r, NH) * 128, 128), 128)
            cot_t[pl.ds(pl.multiple_of(r * 128, 128), 128), :] = cot[:, lanes].T
    halo.wait_recv()
    first_dev = ((z * NX + x) * NC + c) == 0
    for h in range(2):
        got = hr[:, pl.ds(128 * h, 128)].astype(F32)
        gp[h, 0:HALO, :] = jnp.where(first_dev, jnp.zeros_like(got), got)
        conv_rows(h, 0, HALO)
    point_rows(0, HALO)
    y_first = row_sums(0, 1, 1, ys0, yr0)
    yr0[y] = ys0[...]
    rows_c = 64 * 2 * HC

    def c_copy(k):
        return pltpu.make_async_remote_copy(
            w32.at[k, 1 - c], wc.at[k], c_ss, c_rs.at[div(k, 2)], device_id={"c": 1 - c}, device_id_type=MESH)

    @pl.loop(0, CHUNKS)
    def _(k):
        rows = pl.ds(pl.multiple_of(rem(k + 1, CHUNKS) * rows_c, rows_c), rows_c)
        w = lax.dot_general(cot_t[rows, :], hid[...], (((1,), (0,)), ((), ())), preferred_element_type=F32)
        for e in range(HC):
            for pz in range(2):
                for px in range(NX):
                    for pc in range(NC):
                        r = 64 * (2 * e + pz) + 16 * px + 8 * pc
                        for h in range(2):
                            w32[k, pc, pz, px, e, h, :, :] = w[r:r + 8, 128 * h:128 * h + 128]
        c_copy(k).start()

    x_cp = [[pltpu.make_async_remote_copy(
        xs.at[p, 1 - pz, px], xr.at[p, q], x_ss.at[p], x_rs.at[p], device_id=mate(pz, px, c), device_id_type=MESH)
        for pz, px, q in wmates] for p in range(2)]

    def x_phase(p):
        wait_for(wc.at[pl.ds(2 * p, 2)], c_rs.at[p])
        for k in (2 * p, 2 * p + 1):
            for pz in range(2):
                @pl.loop(0, NX)
                def _(px):
                    v = (w32[k, c, pz, px] + wc[k, pz, px]).reshape(HC, 16, 128)
                    xs[p, pz, px, k % 2 * HC:(k % 2 + 1) * HC] = v.astype(BF16)
        for cp in x_cp[p]:
            cp.start()
    heard(1)
    tell(2)
    inv = 1.0 / (NY * pvg.shape[2])

    def d_conv(lo, hi, yr):
        for b in range(lo // 4, (hi + 3) // 4):
            rows = pl.ds(128 * b, 128)
            tot = ((yr[0, b] + yr[1, b]) + (yr[2, b] + yr[3, b])) * inv
            s1[rows, :] = jnp.broadcast_to(tot[0:1, :], (128, 128)).T
            s2[rows, :] = jnp.broadcast_to(tot[1:2, :], (128, 128)).T

        @pl.loop(lo, hi)
        def _(i):
            sl = pl.ds(pl.multiple_of(i * 32, 32), 32)
            for h in range(2):
                dcp[h, sl, :] = rs[sl, :] * (dn[h, sl, :] - s1[sl, :] - nm[h, sl, :] * s2[sl, :])

    def tap_rows(lo, hi, start):
        for h in range(2):
            def step(i, acc):
                acc = list(acc)
                for e in range(4):
                    r0 = pl.multiple_of(i * 32 + 8 * e, 8)
                    d = dcp[h, pl.ds(r0, 8), :]
                    for k in range(taps):
                        acc[k] = acc[k] + d * gp[h, pl.ds(r0 + (HALO + 1 - taps + k), 8), :]
                return tuple(acc)
            init = tuple(jnp.zeros((8, 128), F32) if start else kacc[h, k] for k in range(taps))
            acc = lax.fori_loop(lo, hi, step, init)
            for k in range(taps):
                if start:
                    kacc[h, k] = acc[k]
                else:
                    tp[k // 4, 4 * h + k % 4, :] = jnp.sum(acc[k], axis=0)
    wait_for(yr.at[pl.ds(0, NY - 1)], y_rs.at[0])
    d_conv(1, length // 32, yr)
    tap_rows(1, length // 32, True)
    for h in range(2):
        tp[taps // 4, 4 * h + taps % 4, :] = jnp.sum(gacc[h], axis=0)
    wait_for(yr0.at[pl.ds(0, NY - 1)], y_rs.at[1])
    d_conv(0, 1, yr0)
    dhalo = pltpu.make_async_remote_copy(
        dcp.at[:, pl.ds(0, HALO), :], dcp.at[:, pl.ds(length, HALO), :], dhalo_sem.at[0], dhalo_sem.at[1],
        device_id=prv, device_id_type=MESH)
    tap_rows(0, 1, False)
    t_cp = []
    for pz, px, q in owners:
        t_cp.append(pltpu.make_async_remote_copy(
            tp.at[pz * NX + px], tr.at[8 * c + g_me], t_ss, t_rs, device_id=mate(pz, px, 1), device_id_type=MESH))
    for cp in t_cp[:-1]:
        cp.start()

    @pl.when(c == 0)
    def _():
        t_cp[-1].start()

    @pl.when(c == 1)
    def _():
        tr[8 * c + g_me] = tp[g_me]
    dhalo.start()
    x_phase(0)
    x_phase(1)

    def d_gated(h, r0, rows):
        acc = jnp.zeros((rows, 128), F32)
        for k in range(taps):
            acc = acc + wt[h, k:k + 1, :] * dcp[h, pl.ds(r0 + (taps - 1 - k), rows), :]
        sl, lanes = pl.ds(r0, rows), pl.ds(128 * h, 128)
        s = sg[h, sl, :]
        vg_o[sl, lanes] = (acc * s).astype(BF16)
        gg_o[sl, lanes] = (acc * pvg[0, sl, lanes].astype(F32) * s * (1.0 - s)).astype(BF16)
    @pl.loop(0, 2 * ((length - HALO) // 32))
    def _(i):
        d_gated(rem(i, 2), pl.multiple_of(div(i, 2) * 32, 32), 32)

    def z_copy(src, dst, ss, rs_, d):
        return pltpu.make_async_remote_copy(
            src, dst, ss, rs_, device_id={"z": rem(z + 2 * d + 1 + 2 * (NH - 1) * zp, NZ)}, device_id_type=MESH)

    by_distance = []
    for d in range(NH // 2 - 1, -1, -1):
        by_distance += [NH - 1 - d, d]

    def tree(parts):
        while len(parts) > 1:
            parts = [a + b for a, b in zip(parts[::2], parts[1::2])] + parts[len(parts) // 2 * 2:]
        return parts[0]

    def z_phase(p):
        wait_for(xr.at[p], x_rs.at[p])
        for k in (2 * p, 2 * p + 1):
            v = (w32[k, c, 1 - zp, x] + wc[k, 1 - zp, x]).reshape(HC, 16, 128)
            for q in range(2 * NX - 1):
                v = v + xr[p, q, k % 2 * HC:(k % 2 + 1) * HC].astype(F32)
            r0 = (k + 1) % CHUNKS * HC
            zs[r0:r0 + HC] = v.astype(BF16)
        for d in by_distance:
            if (HC <= d < 3 * HC) == (p == 0):
                z_copy(zs.at[d], zr.at[d], z_ss, z_rs, d).start()
    heard(2)


    @pl.when(c == 1)
    def _():
        wait_for(tr.at[pl.ds(0, 15)], t_rs)
        share = tree([tr[k] for k in range(16)])
        tf[0] = share
        for d in by_distance:
            z_copy(tf.at[0], tz.at[zh], tz_ss, tz_rs, d).start()
    z_phase(0)
    z_phase(1)
    last_dev = ((z * NX + x) * NC + c) == NZ * NX * NC - 1
    dhalo.wait_recv()
    for h in range(2):
        got = dcp[h, pl.ds(length, HALO), :]
        dcp[h, pl.ds(length, HALO), :] = jnp.where(last_dev, jnp.zeros_like(got), got)
        d_gated(h, length - HALO, HALO)

    halo.wait_send()
    dhalo.wait_send()
    wait_for(yr.at[pl.ds(0, NY - 1)], y_ss.at[0])
    wait_for(yr0.at[pl.ds(0, NY - 1)], y_ss.at[1])
    wait_for(wc, c_ss)
    for p in range(2):
        wait_for(xr.at[p], x_ss.at[p])

    @pl.when(c == 0)
    def _():
        wait_for(tp, t_ss)

    @pl.when(c == 1)
    def _():
        wait_for(tp.at[pl.ds(0, 7)], t_ss)

    def f_copy(to):
        return pltpu.make_async_remote_copy(
            tf.at[1], tacc.at[g_sum], tf_ss, tf_rs, device_id=mate(*to), device_id_type=MESH)

    @pl.when(c == 1)
    def _():
        wait_for(tz, tz_rs)
        total = tree([tz[i] for i in range(NH)])
        tf[1] = total
        for to in mates:
            f_copy(to).start()
        tacc[g_sum] = total

    wait_for(zr, z_rs)
    wsum = tree([zr[i].astype(F32) for i in range(NH)])
    for h in range(2):
        wg_o[:, pl.ds(128 * h, 128)] = wsum[8 * h:8 * h + 8, :]
    wait_for(zr, z_ss)

    @pl.when(c == 1)
    def _():
        wait_for(tz, tz_ss)

    @pl.when(c == 0)
    def _():
        wait_for(tacc, tf_rs)

    @pl.when(c == 1)
    def _():
        wait_for(tacc.at[pl.ds(0, 7)], tf_rs)
    for k in range(taps + 1):
        for h in range(2):
            row = tacc[k // 4, 4 * h + k % 4:4 * h + k % 4 + 1, :]
            if k < taps:
                tg_o[k:k + 1, pl.ds(128 * h, 128)] = row
            else:
                gn_o[pl.ds(128 * h, 128)] = row.reshape(128)

    @pl.when(c == 1)
    def _():
        wait_for(tr.at[pl.ds(0, 15)], tf_ss)


def out_kernel(*refs):
    n = len(refs) // 2
    sems = refs[-1]
    cps = [pltpu.make_async_copy(refs[k], refs[n + k], sems.at[k]) for k in range(n)]
    for cp in cps:
        cp.start()
    for cp in cps:
        cp.wait()


def shards(pv, pg, cot, ow, taps, gain, mean, scale):
    length, ch = pv.shape
    d = cot.shape[1]
    blocks = length // 128
    V, D = pltpu.VMEM, pltpu.SemaphoreType.DMA
    any_spec, vmem = pl.BlockSpec(memory_space=pl.ANY), pl.BlockSpec(memory_space=pltpu.VMEM)
    scratch = [
        V((2, length, ch), BF16), V((length, d), BF16), V((ch, d), BF16),
        V(taps.shape, BF16), V((ch,), F32), V((length,), F32), V((length,), F32),
        V((HALO, ch), BF16), V((HALO, ch), BF16),
        V((2, length + HALO, 128), F32), V((2, length, 128), F32), V((2, length, 128), F32),
        V((2, length, 128), F32), V((2, length, 128), F32), V((2, length, 128), F32),
        V((length, ch), BF16), V((2, length + HALO, 128), F32),
        V((length, 128), F32), V((length, 128), F32), V((length, 128), F32), V((length, 128), F32),
        V((2, 32, 128), F32), V((2, 8, 128), F32),
        V((d, length), BF16),
        V((blocks, 2, 128), F32), V((NY, blocks, 2, 128), F32), V((1, 2, 128), F32), V((NY, 1, 2, 128), F32),
        V((2, 32, 8, 128), F32),
        V((8, 8, 128), F32), V((8, 8, 128), F32), V((16, 8, 128), F32), V((NH, 8, 128), F32), V((2, 8, 128), F32),
        V((CHUNKS, NC, 2, NX, HC, 2, 8, 128), F32), V((CHUNKS, 2, NX, HC, 2, 8, 128), F32),
        V((2, 2, NX, NH // 2, 16, 128), BF16), V((2, 2 * NX - 1, NH // 2, 16, 128), BF16),
        V((NH, 16, 128), BF16), V((NH, 16, 128), BF16),
        D((7,)), D((2,)), D((2,)), D((2,)), D((2,)), D, D, D, D, D, D,
        D, D((2,)), D((2,)), D((2,)), D, D,
        pltpu.SemaphoreType.REGULAR((3,)),
    ]
    outs = (((length, ch), BF16), ((length, ch), BF16), ((8, ch), F32), (taps.shape, F32), ((ch,), F32))
    res = pl.pallas_call(
        main_kernel,
        out_shape=tuple(V(s, t) for s, t in outs),
        in_specs=[any_spec] * 8,
        out_specs=(vmem,) * 5,
        scratch_shapes=scratch,
        name="conv_back",
        compiler_params=pltpu.CompilerParams(collective_id=0, has_side_effects=True, vmem_limit_bytes=56 * 2**20),
    )(pv, pg, cot, ow, taps, gain, mean, scale)
    return pl.pallas_call(
        out_kernel,
        out_shape=tuple(jax.ShapeDtypeStruct(s, t) for s, t in outs),
        in_specs=[vmem] * 5,
        out_specs=(any_spec,) * 5,
        scratch_shapes=[D((5,))],
        name="write_out",
    )(*(pltpu.with_memory_space_constraint(r, pltpu.VMEM) for r in res))


def solution(mesh):
    split = Mesh(mesh.devices.reshape(NZ, NX, NC, mesh.shape["tp"]), ("z", "x", "c", "y"))
    placed = (P(SP, "y"), P(SP, "y"), P(SP, None), P("y", None), P(None, "y"), P("y"), P(SP), P(SP))
    return jax.shard_map(
        shards, mesh=split, in_specs=placed,
        out_specs=(P(SP, "y"), P(SP, "y"), P(SP, "y"), P(None, "y"), P("y")), check_vma=False,
    )
```

time: 53.9 us -> 50.9 us (0.944)
  Pallas kernels: 53.1 us -> 50.1 us
    pallas_call x1, Pallas kernels: 52.3 us -> 49.3 us  [shards(): pl.pallas_call(main_kernel, out_shape=tuple((V(s, t) for s, t in outs)),...]
where the time goes in v4:
time: 50.9 us; the launch traced here: 50.8 us
  Pallas kernels  50.1 us (98%)
  between operations  0.64 us (1%)
    pallas_call x1, Pallas kernels, shards(): pl.pallas_call(main_kernel, out_shape=tuple((V(s, t) for s, t in outs)),...  49.3 us

profile of v4, /device:TPU:1, one launch (start us, length us, event | category | flops | bytes accessed | tf_op | source)
XLA Modules:
  0.0 50.8 jit_solution(5109108236499783847)
XLA Ops:
  0.6 49.3 %conv_back.1 = (bf16[384,256]{1,0:T(8,128)(2,1)S(1)}, bf16[384,256]{1,0:T(8,128)(2,1)S(1)}, f32[8,256]{1,0:T(8,128)S(1)}, f32[31,256]{1,0:T(8,128)S(1)}, f32[256]{0:T(256)S(1)}) custom-call(bf16[384,256]{1,0:T(8,128)(2,1)} %pv_h.1, bf16[384,256]{1,0:T(8,128)(2,1)} %pg_h.1, bf16[384,2048]{1,0:T(8,128)(2,1)} %cot_h.1, bf16[256,2048]{1,0:T(8,128)(2,1)} %ow_h.1, ...), custom_call_target="tpu_custom_call" | custom-call | tf_op jit(solution)/shard_map/conv_back/pallas_call | solution.py:446
  50.0 0.8 %write_out.1 = (bf16[384,256]{1,0:T(8,128)(2,1)}, bf16[384,256]{1,0:T(8,128)(2,1)}, f32[8,256]{1,0:T(8,128)}, f32[31,256]{1,0:T(8,128)}, f32[256]{0:T(256)}) custom-call(bf16[384,256]{1,0:T(8,128)(2,1)S(1)} %get-tuple-element.10.refs_0_, bf16[384,256]{1,0:T(8,128)(2,1)S(1)} %get-tuple-element.11.refs_1_, f32[8,256]{1,0:T(8,128)S(1)} %get-tuple-element.12.refs_2_, ...), custom_call_target="tpu_custom_call" | custom-call | tf_op jit(solution)/shard_map/write_out/pallas_call | solution.py:455

commit v5 on v4

--- a/solution.py
+++ b/solution.py
@@ -16,6 +16,7 @@
 NH = NZ // 2
 CHUNKS = 4
 HC = NH // CHUNKS
+EARLY, FIRST = 12, 2 * HC
 
 
 def sigmoid(v):
@@ -27,7 +28,7 @@
     vg_o, gg_o, wg_o, tg_o, gn_o,
     pvg, cot, ow, taps_b, gain_v, mean_v, scale_v,
     hs, hr, gp, sg, us, cv, nm, dn, hid, dcp, rm, rs, s1, s2, wt, gacc,
-    cot_t, ys, yr, ys0, yr0, kacc, tacc, tp, tr, tz, tf, w32, wc, xs, xr, zs, zr,
+    cot_t, ys, yr, ys0, yr0, kacc, tacc, tp, tr, tz, tf, w32, wc, xs0, xs1, xr0, xr1, zs, zr,
     in_sem, halo_sem, dhalo_sem, y_ss, y_rs, t_ss, t_rs, tz_ss, tz_rs, tf_ss, tf_rs,
     c_ss, c_rs, x_ss, x_rs, z_ss, z_rs, far_sem,
 ):
@@ -185,7 +186,7 @@
     def _(i):
         for e in range(2):
             r = 2 * i + e
-            lanes = pl.ds(pl.multiple_of(rem(zh + r, NH) * 128, 128), 128)
+            lanes = pl.ds(pl.multiple_of(r * 128, 128), 128)
             cot_t[pl.ds(pl.multiple_of(r * 128, 128), 128), :] = cot[:, lanes].T
     halo.wait_recv()
     first_dev = ((z * NX + x) * NC + c) == 0
@@ -200,11 +201,11 @@
 
     def c_copy(k):
         return pltpu.make_async_remote_copy(
-            w32.at[k, 1 - c], wc.at[k], c_ss, c_rs.at[div(k, 2)], device_id={"c": 1 - c}, device_id_type=MESH)
+            w32.at[k, 1 - c], wc.at[k], c_ss, c_rs.at[div(k + CHUNKS - 2, CHUNKS - 1)], device_id={"c": 1 - c}, device_id_type=MESH)
 
     @pl.loop(0, CHUNKS)
     def _(k):
-        rows = pl.ds(pl.multiple_of(rem(k + 1, CHUNKS) * rows_c, rows_c), rows_c)
+        rows = pl.ds(pl.multiple_of(k * rows_c, rows_c), rows_c)
         w = lax.dot_general(cot_t[rows, :], hid[...], (((1,), (0,)), ((), ())), preferred_element_type=F32)
         for e in range(HC):
             for pz in range(2):
@@ -215,22 +216,25 @@
                             w32[k, pc, pz, px, e, h, :, :] = w[r:r + 8, 128 * h:128 * h + 128]
         c_copy(k).start()
 
+    parts = ((xs0, xr0, 0, 1), (xs1, xr1, 1, CHUNKS))
     x_cp = [[pltpu.make_async_remote_copy(
-        xs.at[p, 1 - pz, px], xr.at[p, q], x_ss.at[p], x_rs.at[p], device_id=mate(pz, px, c), device_id_type=MESH)
-        for pz, px, q in wmates] for p in range(2)]
+        xs.at[1 - pz, px], xr.at[q], x_ss.at[p], x_rs.at[p], device_id=mate(pz, px, c), device_id_type=MESH)
+        for pz, px, q in wmates] for p, (xs, xr, _, _) in enumerate(parts)]
 
     def x_phase(p):
-        wait_for(wc.at[pl.ds(2 * p, 2)], c_rs.at[p])
-        for k in (2 * p, 2 * p + 1):
+        xs, xr, lo, hi = parts[p]
+        wait_for(wc.at[pl.ds(lo, hi - lo)], c_rs.at[p])
+        for k in range(lo, hi):
             for pz in range(2):
                 @pl.loop(0, NX)
                 def _(px):
                     v = (w32[k, c, pz, px] + wc[k, pz, px]).reshape(HC, 16, 128)
-                    xs[p, pz, px, k % 2 * HC:(k % 2 + 1) * HC] = v.astype(BF16)
+                    xs[pz, px, (k - lo) * HC:(k - lo + 1) * HC] = v.astype(BF16)
         for cp in x_cp[p]:
             cp.start()
     heard(1)
     tell(2)
+
     inv = 1.0 / (NY * pvg.shape[2])
 
     def d_conv(lo, hi, yr):
@@ -289,8 +293,15 @@
     def _():
         tr[8 * c + g_me] = tp[g_me]
     dhalo.start()
+
+    early = z < EARLY
+    late = jnp.logical_not(early)
     x_phase(0)
-    x_phase(1)
+
+    @pl.when(early)
+    def _():
+        x_phase(1)
+
 
     def d_gated(h, r0, rows):
         acc = jnp.zeros((rows, 128), F32)
@@ -306,11 +317,7 @@
 
     def z_copy(src, dst, ss, rs_, d):
         return pltpu.make_async_remote_copy(
-            src, dst, ss, rs_, device_id={"z": rem(z + 2 * d + 1 + 2 * (NH - 1) * zp, NZ)}, device_id_type=MESH)
-
-    by_distance = []
-    for d in range(NH // 2 - 1, -1, -1):
-        by_distance += [NH - 1 - d, d]
+            src, dst, ss, rs_, device_id={"z": 2 * d + 1 - zp}, device_id_type=MESH)
 
     def tree(parts):
         while len(parts) > 1:
@@ -318,16 +325,19 @@
         return parts[0]
 
     def z_phase(p):
-        wait_for(xr.at[p], x_rs.at[p])
-        for k in (2 * p, 2 * p + 1):
+        xs, xr, lo, hi = parts[p]
+        wait_for(xr, x_rs.at[p])
+        for k in range(lo, hi):
             v = (w32[k, c, 1 - zp, x] + wc[k, 1 - zp, x]).reshape(HC, 16, 128)
             for q in range(2 * NX - 1):
-                v = v + xr[p, q, k % 2 * HC:(k % 2 + 1) * HC].astype(F32)
-            r0 = (k + 1) % CHUNKS * HC
-            zs[r0:r0 + HC] = v.astype(BF16)
-        for d in by_distance:
-            if (HC <= d < 3 * HC) == (p == 0):
-                z_copy(zs.at[d], zr.at[d], z_ss, z_rs, d).start()
+                v = v + xr[q, (k - lo) * HC:(k - lo + 1) * HC].astype(F32)
+            zs[k * HC:(k + 1) * HC] = v.astype(BF16)
+        for d in range(lo * HC, hi * HC):
+            z_copy(zs.at[d], zr.at[zh], z_ss, z_rs, d).start()
+
+    def share_out(lo, hi):
+        for d in range(lo, hi):
+            z_copy(tf.at[0], tz.at[zh], tz_ss, tz_rs, d).start()
     heard(2)
 
 
@@ -336,16 +346,31 @@
         wait_for(tr.at[pl.ds(0, 15)], t_rs)
         share = tree([tr[k] for k in range(16)])
         tf[0] = share
-        for d in by_distance:
-            z_copy(tf.at[0], tz.at[zh], tz_ss, tz_rs, d).start()
+        share_out(0, FIRST)
     z_phase(0)
-    z_phase(1)
+    @pl.when(early)
+    def _():
+        z_phase(1)
+
+    @pl.when((c == 1) & early)
+    def _():
+        share_out(FIRST, NH)
+    @pl.when(late)
+    def _():
+        x_phase(1)
     last_dev = ((z * NX + x) * NC + c) == NZ * NX * NC - 1
     dhalo.wait_recv()
     for h in range(2):
         got = dcp[h, pl.ds(length, HALO), :]
         dcp[h, pl.ds(length, HALO), :] = jnp.where(last_dev, jnp.zeros_like(got), got)
         d_gated(h, length - HALO, HALO)
+    @pl.when(late)
+    def _():
+        z_phase(1)
+
+    @pl.when((c == 1) & late)
+    def _():
+        share_out(FIRST, NH)
 
     halo.wait_send()
     dhalo.wait_send()
@@ -353,7 +378,7 @@
     wait_for(yr0.at[pl.ds(0, NY - 1)], y_ss.at[1])
     wait_for(wc, c_ss)
     for p in range(2):
-        wait_for(xr.at[p], x_ss.at[p])
+        wait_for(parts[p][1], x_ss.at[p])
 
     @pl.when(c == 0)
     def _():
@@ -436,7 +461,8 @@
         V((2, 32, 8, 128), F32),
         V((8, 8, 128), F32), V((8, 8, 128), F32), V((16, 8, 128), F32), V((NH, 8, 128), F32), V((2, 8, 128), F32),
         V((CHUNKS, NC, 2, NX, HC, 2, 8, 128), F32), V((CHUNKS, 2, NX, HC, 2, 8, 128), F32),
-        V((2, 2, NX, NH // 2, 16, 128), BF16), V((2, 2 * NX - 1, NH // 2, 16, 128), BF16),
+        V((2, NX, HC, 16, 128), BF16), V((2, NX, NH - HC, 16, 128), BF16),
+        V((2 * NX - 1, HC, 16, 128), BF16), V((2 * NX - 1, NH - HC, 16, 128), BF16),
         V((NH, 16, 128), BF16), V((NH, 16, 128), BF16),
         D((7,)), D((2,)), D((2,)), D((2,)), D((2,)), D, D, D, D, D, D,
         D, D((2,)), D((2,)), D((2,)), D, D,

time: 50.9 us -> 49.7 us (0.976)
  Pallas kernels: 50.1 us -> 48.9 us
    pallas_call x1, Pallas kernels: 49.3 us -> 48.1 us  [shards(): pl.pallas_call(main_kernel, out_shape=tuple((V(s, t) for s, t in outs)),...]
where the time goes in v5:
time: 49.7 us; the launch traced here: 49.6 us
  Pallas kernels  48.9 us (98%)
  between operations  0.64 us (1%)
    pallas_call x1, Pallas kernels, shards(): pl.pallas_call(main_kernel, out_shape=tuple((V(s, t) for s, t in outs)),...  48.1 us

profile of v5, /device:TPU:1, one launch (start us, length us, event | category | flops | bytes accessed | tf_op | source)
XLA Modules:
  0.0 49.6 jit_solution(8434836961020180743)
XLA Ops:
  0.6 48.1 %conv_back.1 = (bf16[384,256]{1,0:T(8,128)(2,1)S(1)}, bf16[384,256]{1,0:T(8,128)(2,1)S(1)}, f32[8,256]{1,0:T(8,128)S(1)}, f32[31,256]{1,0:T(8,128)S(1)}, f32[256]{0:T(256)S(1)}) custom-call(bf16[384,256]{1,0:T(8,128)(2,1)} %pv_h.1, bf16[384,256]{1,0:T(8,128)(2,1)} %pg_h.1, bf16[384,2048]{1,0:T(8,128)(2,1)} %cot_h.1, bf16[256,2048]{1,0:T(8,128)(2,1)} %ow_h.1, ...), custom_call_target="tpu_custom_call" | custom-call | tf_op jit(solution)/shard_map/conv_back/pallas_call | solution.py:472
  48.8 0.8 %write_out.1 = (bf16[384,256]{1,0:T(8,128)(2,1)}, bf16[384,256]{1,0:T(8,128)(2,1)}, f32[8,256]{1,0:T(8,128)}, f32[31,256]{1,0:T(8,128)}, f32[256]{0:T(256)}) custom-call(bf16[384,256]{1,0:T(8,128)(2,1)S(1)} %get-tuple-element.10.refs_0_, bf16[384,256]{1,0:T(8,128)(2,1)S(1)} %get-tuple-element.11.refs_1_, f32[8,256]{1,0:T(8,128)S(1)} %get-tuple-element.12.refs_2_, ...), custom_call_target="tpu_custom_call" | custom-call | tf_op jit(solution)/shard_map/write_out/pallas_call | solution.py:481
